TPU v7x, 256 devices: a whole 4x4x8 slice. The times are simulated.
256 devices in a mesh: ep: 64 (over z, y, core), tp: 4 (over x).
Axes of the slice: x: 4, y: 4, z: 8, core: 2. Of those that a mesh axis runs over, the one named last changes fastest.
Arguments:
- queries: bfloat16 [16384, 8, 128], P('ep', 'tp'), may hold values from -15 to 15
- keys: bfloat16 [16384, 4, 128], P('ep', 'tp'), may hold values from -6 to 6
- values: bfloat16 [16384, 4, 128], P('ep', 'tp'), may hold values from -6 to 6
- key_bias: bfloat16 [16384, 8], P('ep', 'tp'), may hold values from -20 to 2
- out_weight: bfloat16 [1024, 2048], P('tp'), may hold values from -0.1875 to 0.1875
- tokens_b: bfloat16 [32768, 2048], P(('ep', 'tp')), may hold values from -6 to 6
- moe_gain: bfloat16 [2048], replicated, may hold values from 0.099609375 to 1.8984375
- gate_weight: bfloat16 [64, 2048, 2048], P('ep', None, 'tp'), may hold values from -0.125 to 0.125
- up_weight: bfloat16 [64, 2048, 2048], P('ep', None, 'tp'), may hold values from -0.125 to 0.125
- down_weight: bfloat16 [64, 2048, 2048], P('ep', 'tp'), may hold values from -0.125 to 0.125
- routes: int32 [32768, 2], P(('ep', 'tp')), may hold values from 0 to 63, all different within a row; in each aligned block of 128 rows (0 to 127, 128 to 255, ...) at most 6 rows name the same one
- route_weights: float32 [32768, 2], P(('ep', 'tp')), may hold values from 0.2 to 1
Outputs:
- mixed: bfloat16 [16384, 2048], P(('ep', 'tp'))
- moe_out: bfloat16 [32768, 2048], P(('ep', 'tp'))
Inputs may be any that keep to these rules, and one draw needn't show every extreme that they name: `routes`: each row names 2 different experts. In each aligned block of 128 rows (the rows of one device) no expert is named by more than 6 rows, and in some block one expert is named by exactly 6 rows.
All inputs are finite; a program needn't handle non-finite values.
Results may differ from a plain program's by a relative error of at most 0.012.
Values may be sent and summed in bfloat16 or wider, within the bound.
A program may use at most 128 MiB of HBM per device.

v0:
```python
import math

import jax
import jax.numpy as jnp
from jax import lax
from jax.sharding import PartitionSpec as P


def in_one_piece(arrays, axis, dim, along):
    columns = [a.reshape(*a.shape[:along], -1) for a in arrays]
    both = jnp.concatenate(columns, axis=along)
    filled, at, done = (lax.all_gather(both, axis, axis=dim, tiled=True), 0, [])
    for a, column in zip(arrays, columns):
        share = filled[..., at : at + column.shape[along]]
        done.append(share.reshape(*share.shape[:along], *a.shape[along:]))
        at += column.shape[along]
    return tuple(done)


def partner(value, axis, apart):
    mask = 2**apart
    pairs = [(source, source ^ mask) for source in range(lax.axis_size(axis))]
    return lax.ppermute(value, axis, pairs)


def split_up(value, dim, length):
    before, after = (value.shape[:dim], value.shape[dim + 1 :])
    return jnp.moveaxis(value.reshape(*before, length, -1, *after), dim, 0)


def summed_on_arrival(value, axis, dim):
    pieces = split_up(value, dim, lax.axis_size(axis))
    arrived = lax.all_to_all(pieces, axis, split_axis=0, concat_axis=0, tiled=True)
    return arrived.astype(jnp.float32).sum(axis=0)


def entry_slots(routes, expert_total):
    flattened_expert_list = routes.reshape(-1)
    onehot = (
        flattened_expert_list[:, None] == jnp.arange(expert_total, dtype=jnp.int32)[None, :]
    ).astype(jnp.int32)
    earlier_count = jnp.cumsum(onehot, axis=0) - onehot
    return (flattened_expert_list, jnp.sum(earlier_count * onehot, axis=1))


def swiglu_rows(piece, gate_cols, up_cols):
    gate_val = jnp.dot(piece, gate_cols, preferred_element_type=jnp.float32)
    up_val = jnp.dot(piece, up_cols, preferred_element_type=jnp.float32)
    return (jax.nn.silu(gate_val) * up_val).astype(jnp.bfloat16)


def attend_rows(query_block, first_pos, keys_all, values_all, bias_all, local_kv):
    row_count, local_heads, head_dim = query_block.shape
    group_size = local_heads // local_kv
    key_total = keys_all.shape[0]
    key_span = min(1024, key_total)
    query_pos = first_pos + jnp.arange(row_count, dtype=jnp.int32)
    query_rows = query_block.reshape(row_count, local_kv, group_size, head_dim)
    visit_total = (first_pos + row_count + key_span - 1) // key_span
    score_scale = 1.0 / math.sqrt(head_dim)

    def visit(visit_no, state):
        accum, carried = state
        begin_at = (visit_total - 1 - visit_no) * key_span
        key_tile_rows = lax.dynamic_slice_in_dim(keys_all, begin_at, key_span, 0)
        value_block = lax.dynamic_slice_in_dim(values_all, begin_at, key_span, 0)
        bias_block = (
            lax.dynamic_slice_in_dim(bias_all, begin_at, key_span, 0)
            .astype(jnp.float32)
            .reshape(key_span, local_kv, group_size)
        )
        scores = (
            jnp.einsum(
                "rkgd,skd->kgrs", query_rows, key_tile_rows, preferred_element_type=jnp.float32
            )
            * score_scale
        )
        scores = scores + jnp.transpose(bias_block, (1, 2, 0))[:, :, None, :]
        key_pos = begin_at + jnp.arange(key_span, dtype=jnp.int32)
        earlier = key_pos[None, :] < query_pos[:, None]
        log_keep = jnp.where(earlier, jax.nn.log_sigmoid(-scores), 0.0)
        after = lax.cumsum(log_keep, axis=3, reverse=True) - log_keep
        weights = jnp.where(
            earlier, jnp.exp(jax.nn.log_sigmoid(scores) + after + carried[..., None]), 0.0
        ).astype(jnp.bfloat16)
        accum = accum + jnp.einsum(
            "kgrs,skd->kgrd", weights, value_block, preferred_element_type=jnp.float32
        )
        return (accum, carried + jnp.sum(log_keep, axis=3))

    start_state = (
        jnp.zeros((local_kv, group_size, row_count, head_dim), jnp.float32),
        jnp.zeros((local_kv, group_size, row_count), jnp.float32),
    )
    accum = lax.fori_loop(0, visit_total, visit, start_state)[0]
    return (
        jnp.transpose(accum, (2, 0, 1, 3))
        .reshape(row_count, local_heads * head_dim)
        .astype(jnp.bfloat16)
    )


def body(
    queries,
    keys,
    values,
    key_bias,
    out_weight,
    tokens_b,
    moe_gain,
    gate_weight,
    up_weight,
    down_weight,
    routes,
    route_weights,
):
    tok_rows, local_heads, head_dim = queries.shape
    local_kv = keys.shape[1]
    ep_count = lax.axis_size("ep")
    keys_all, values_all, bias_all = in_one_piece((keys, values, key_bias), "ep", 0, 1)
    device_ep = lax.axis_index("ep")
    half_rows = tok_rows // 2
    bit_count = ep_count.bit_length() - 1
    handed = queries[half_rows:]
    for bit_no in range(bit_count):
        handed = partner(handed, "ep", bit_no)
    companion_batch = ep_count - 1 - device_ep
    own_part = attend_rows(
        queries[:half_rows], device_ep * tok_rows, keys_all, values_all, bias_all, local_kv
    )
    other_part = attend_rows(
        handed, companion_batch * tok_rows + half_rows, keys_all, values_all, bias_all, local_kv
    )
    for bit_no in range(bit_count):
        other_part = partner(other_part, "ep", bit_no)
    attended = jnp.concatenate((own_part, other_part), axis=0)
    tok_b, model_width = tokens_b.shape
    top_count = routes.shape[1]
    expert_total = ep_count * gate_weight.shape[0]
    capacity = max(2, 3 * top_count * tok_b // (2 * expert_total))
    tokens_f = tokens_b.astype(jnp.float32)
    normed = (
        tokens_f
        * lax.rsqrt(jnp.mean(tokens_f * tokens_f, axis=1, keepdims=True) + 1e-06)
        * moe_gain.astype(jnp.float32)
    ).astype(jnp.bfloat16)
    flattened_expert_list, slot_index = entry_slots(routes, expert_total)
    place = flattened_expert_list * capacity + slot_index
    outbound = (
        jnp.zeros((expert_total * capacity, model_width), jnp.bfloat16)
        .at[place]
        .set(jnp.repeat(normed, top_count, axis=0))
    )
    outbound = outbound.reshape(expert_total, capacity, model_width)
    gate_cols = gate_weight[0]
    up_cols = up_weight[0]
    down_rows = down_weight[0]
    arrived = lax.all_to_all(outbound, "ep", split_axis=0, concat_axis=0, tiled=True)
    hidden = swiglu_rows(
        lax.all_gather(arrived.reshape(ep_count * capacity, model_width), "tp", axis=0, tiled=True),
        gate_cols,
        up_cols,
    )
    mixed_sum = lax.psum_scatter(
        jnp.dot(attended, out_weight, preferred_element_type=jnp.float32).astype(jnp.bfloat16),
        "tp",
        scatter_dimension=0,
        tiled=True,
    )
    expert_sum = summed_on_arrival(
        jnp.dot(hidden, down_rows, preferred_element_type=jnp.float32).astype(jnp.bfloat16), "tp", 0
    )
    returned = lax.all_to_all(
        expert_sum.astype(jnp.bfloat16).reshape(ep_count, capacity, model_width),
        "ep",
        split_axis=0,
        concat_axis=0,
        tiled=True,
    )
    picked = jnp.take(returned.reshape(expert_total * capacity, model_width), place, axis=0).astype(
        jnp.float32
    )
    weighted = picked * route_weights.reshape(-1)[:, None]
    moe_out = jnp.sum(weighted.reshape(tok_b, top_count, model_width), axis=1).astype(jnp.bfloat16)
    return (mixed_sum, moe_out)


def solution(mesh):
    in_specs = (
        P("ep", "tp", None),
        P("ep", "tp", None),
        P("ep", "tp", None),
        P("ep", "tp"),
        P("tp", None),
        P(("ep", "tp"), None),
        P(),
        P("ep", None, "tp"),
        P("ep", None, "tp"),
        P("ep", "tp", None),
        P(("ep", "tp"), None),
        P(("ep", "tp"), None),
    )
    out_specs = (P(("ep", "tp"), None), P(("ep", "tp"), None))
    return jax.shard_map(body, mesh=mesh, in_specs=in_specs, out_specs=out_specs, check_vma=False)
```

profile of v0, /device:TPU:64, one launch (start us, length us, event | category | flops | bytes accessed | tf_op | source)
XLA Modules:
  0.0 583.1 jit_solution(1064137814376958959)
XLA Ops:
  15.4 4.1 scatter_custom_fusion
  19.5 3.7 reshape.326
  23.2 61.3 %all_to_all.15 = bf16[64,6,2048]{2,1,0:T(8,128)(2,1)} all-to-all(bf16[64,6,2048]{2,1,0:T(8,128)(2,1)} %reshape.326), channel_id=1, replica_groups=mesh['ep'=64,'tp'=4] {'ep'}, dimensions={0} | all-to-all | bytes 3145728 | tf_op jit(solution)/shard_map/all_to_all | solution.py:158
  84.5 3.8 reshape.327
  91.2 3.8 collective-permute-done.1
  97.0 3.8 collective-permute-done.2
  101.8 3.5 collective-permute-done.3
  106.9 3.5 collective-permute-done.4
  110.4 4.0 collective-permute-start.5
  114.5 39.8 %all-gather.5.cloned.1.call-done = bf16[1536,2048]{1,0:T(8,128)(2,1)} async-done(((bf16[384,2048]{1,0:T(8,128)(2,1)}), bf16[1536,2048]{1,0:T(8,128)(2,1)}) %all-gather.5.cloned.1.call-update) | async-done | bytes 6291472 | tf_op jit(solution)/shard_map/all_gather | solution.py:160
  154.3 8.6 %fusion.53 = f32[1536,512]{1,0:T(8,128)} fusion(bf16[1536,2048]{1,0:T(8,128)(2,1)} %all-gather.5.cloned.1.call-done, bf16[1,2048,512]{2,1,0:T(8,128)(2,1)} %param.23), kind=kOutput, calls=%fused_computation.82 | convolution fusion | flops 3221225472 | bytes 11534336 | tf_op jit(solution)/shard_map/dot_general | solution.py:47
  162.9 11.8 %convolution_convert_fusion = bf16[1536,2048]{1,0:T(8,128)(2,1)} fusion(bf16[1,512,2048]{2,1,0:T(8,128)(2,1)S(1)} %copy-done, bf16[1536,2048]{1,0:T(8,128)(2,1)} %all-gather.5.cloned.1.call-done, f32[1536,512]{1,0:T(8,128)} %fusion.53, bf16[1,2048,512]{2,1,0:T(8,128)(2,1)} %param.24), kind=kOutput, calls=%fused_computation.74 | convolution fusion | flops 6450315264 | bytes 19922944 | tf_op jit(solution)/shard_map/dot_general | solution.py:171
  174.7 5.2 all-to-all-start.1
  179.9 67.3 %all-gather.3.cloned.1.call-done = bf16[16384,258]{1,0:T(8,128)(2,1)} async-done(((bf16[256,258]{1,0:T(8,128)(2,1)}), bf16[16384,258]{1,0:T(8,128)(2,1)}) %all-gather.3.cloned.1.call-update) | async-done | bytes 8454160 | tf_op jit(solution)/shard_map/all_gather | solution.py:12
  247.2 5.7 slice_bitcast_fusion.4
  252.9 3.8 slice.59
  256.7 3.7 copy.53
  260.5 94.1 %while.31 = (s32[]{:T(128)}, f32[1,2,128,128]{3,2,1,0:T(8,128)S(1)}, f32[1,2,128]{2,1,0:T(2,128)S(1)}, s32[]{:T(128)}, s32[]{:T(128)}, /*index=5*/bf16[16384,1,1...) while((s32[]{:T(128)}, ...), condition=%wide.region_9.10_spmd.clone, body=%wide.region_5.9_spmd.clone.sunk | while | flops 176343936 | bytes 10775775 | solution.py:95
  262.7 2.5 fusion.100
  270.5 2.5 fusion.100
  278.4 2.5 fusion.100
  286.2 2.5 fusion.100
  294.1 2.5 fusion.100
  301.9 2.5 fusion.100
  309.7 2.5 fusion.100
  317.6 2.5 fusion.100
  325.4 2.5 fusion.100
  333.3 2.5 fusion.100
  341.1 2.5 fusion.100
  349.0 2.5 fusion.100
  356.5 4.1 collective-permute-done.7
  360.6 5.8 collective-permute-done.8
  366.3 4.3 collective-permute-done.9
  370.6 32.4 %collective-permute-start.10 = (bf16[128,256]{0,1:T(8,128)(2,1)S(1)}, bf16[128,256]{0,1:T(8,128)(2,1)S(1)}, u32[]{:S(2)}, u32[]{:S(2)}) collective-permute-start(bf16[128,256]{0,1:T(8,128)(2,1)S(1)} %collective-permute-done.9), channel_id=1, source_target_pairs={{0,64},{4,68},{8,72},{12,76},{16,80},{20,84},{24,88},{28,92},{32,9... | collective-permute-start | bytes 196616 | tf_op jit(solution)/shard_map/ppermute | solution.py:23
  405.4 4.2 reduce_sum.69
  411.2 11.2 %all-to-all-start.2 = ((bf16[64,6,2048]{2,1,0:T(8,128)(2,1)}), bf16[64,6,2048]{2,1,0:T(8,128)(2,1)}, u32[]{:S(2)}, u32[]{:S(2)}) async-start(bf16[64,6,2048]{2,1,0:T(8,128)(2,1)} %reshape.329), calls=%async_computation.3 | async-start | bytes 4194304 | tf_op jit(solution)/shard_map/all_to_all | solution.py:173
  422.4 39.5 %while.30 = (s32[]{:T(128)}, f32[1,2,128,128]{3,2,1,0:T(8,128)S(1)}, f32[1,2,128]{2,1,0:T(2,128)S(1)}, s32[]{:T(128)}, s32[]{:T(128)}, /*index=5*/bf16[16384,1,1...) while((s32[]{:T(128)}, ...), condition=%wide.region_4.5_spmd.clone, body=%wide.region_0.4_spmd.clone.sunk | while | flops 176343936 | bytes 10775775 | solution.py:95
  424.6 2.5 fusion.93
  432.5 2.5 fusion.93
  440.3 2.5 fusion.93
  448.2 2.5 fusion.93
  456.0 2.5 fusion.93
  462.1 2.7 convolution_convert_fusion.1
  465.3 6.9 %all-to-all-done.2 = bf16[64,6,2048]{2,1,0:T(8,128)(2,1)} async-done(((bf16[64,6,2048]{2,1,0:T(8,128)(2,1)}), bf16[64,6,2048]{2,1,0:T(8,128)(2,1)}, u32[]{:S(2)}, u32[]{:S(2)}) %all-to-all-start.2) | async-done | bytes 1572896 | tf_op jit(solution)/shard_map/all_to_all | solution.py:173
  472.2 3.7 reshape.330
  475.9 4.1 gather_fusion
  481.5 6.2 %multiply_reduce_fusion = bf16[128,2048]{1,0:T(8,128)(2,1)} fusion(bf16[128,2,2048]{2,1,0:T(2,128)(2,1)} %gather.7, pred[128,2]{1,0:T(8,128)(4,1)S(1)} %copy.62, f32[128,2]{1,0:T(8,128)S(1)} %copy.64), kind=kLoop, calls=%fused_computation.84 | loop fusion | flops 1835008 | bytes 1574144 | tf_op jit(solution)/shard_map/reduce_sum | solution.py:184
  487.8 88.3 %reduce-scatter.2.cloned.1.call-done = bf16[64,2048]{1,0:T(8,128)(2,1)} async-done(((bf16[256,2048]{1,0:T(8,128)(2,1)}), bf16[64,2048]{1,0:T(8,128)(2,1)}) %reduce-scatter.2.cloned.1.call-update) | async-done | bytes 262160 | tf_op jit(solution)/shard_map/reduce_scatter | solution.py:164
  (280 shorter events, 112.2 us)
Async XLA Ops:
  7.2 155.8 %copy-start = (bf16[1,512,2048]{2,1,0:T(8,128)(2,1)S(1)}, bf16[1,512,2048]{2,1,0:T(8,128)(2,1)}, u32[]{:S(2)}) copy-start(bf16[1,512,2048]{2,1,0:T(8,128)(2,1)} %param.25) | copy-start | bytes 6291460
  7.2 147.1 %all-gather.5.cloned.1.call-start = ((), (), s32[]{:S(2)}) async-start(), calls=%async_computation.6 | async-start | bytes 7864320 | tf_op jit(solution)/shard_map/all_gather | solution.py:160
  84.5 3.8 copy-start.6
  84.5 4.0 copy-start.3
  84.5 4.0 copy-start.4
  84.5 4.7 copy-start.2
  88.3 158.9 %all-gather.3.cloned.1.call-start = ((), (), s32[]{:S(2)}) async-start(), calls=%async_computation.4 | async-start | bytes 12779520 | tf_op jit(solution)/shard_map/all_gather | solution.py:12
  89.4 1.3 collective-permute-start
  90.7 4.3 collective-permute-start.1
  95.0 5.8 collective-permute-start.2
  100.8 4.5 collective-permute-start.3
  105.3 5.2 collective-permute-start.4
  110.4 150.0 %collective-permute-start.5 = (bf16[128,2,128]{2,0,1:T(8,128)(2,1)S(1)}, bf16[128,2,128]{2,0,1:T(8,128)(2,1)S(1)}, u32[]{:S(2)}, u32[]{:S(2)}) collective-permute-start(bf16[128,2,128]{2,0,1:T(8,128)(2,1)S(1)} %collective-permute-done.4), channel_id=1, source_target_pairs={{0,128},{4,132},{8,136},{12,140},{16,144},{20,148},{24,152},{28,15... | collective-permute-start | bytes 196616 | tf_op jit(solution)/shard_map/ppermute | solution.py:23
  174.7 230.7 %all-to-all-start.1 = ((bf16[4,384,2048]{2,1,0:T(8,128)(2,1)}), bf16[4,384,2048]{2,1,0:T(8,128)(2,1)}, u32[]{:S(2)}, u32[]{:S(2)}) async-start(bf16[4,384,2048]{2,1,0:T(8,128)(2,1)} %bitcast.212), calls=%async_computation.2 | async-start | bytes 12582912 | tf_op jit(solution)/shard_map/all_to_all | solution.py:33
  354.8 1.3 collective-permute-start.6
  356.1 4.5 collective-permute-start.7
  360.6 5.8 collective-permute-start.8
  366.3 4.3 collective-permute-start.9
  370.6 34.8 %collective-permute-start.10 = (bf16[128,256]{0,1:T(8,128)(2,1)S(1)}, bf16[128,256]{0,1:T(8,128)(2,1)S(1)}, u32[]{:S(2)}, u32[]{:S(2)}) collective-permute-start(bf16[128,256]{0,1:T(8,128)(2,1)S(1)} %collective-permute-done.9), channel_id=1, source_target_pairs={{0,64},{4,68},{8,72},{12,76},{16,80},{20,84},{24,88},{28,92},{32,9... | collective-permute-start | bytes 196616 | tf_op jit(solution)/shard_map/ppermute | solution.py:23
  405.4 56.7 %collective-permute-start.11 = (bf16[128,256]{0,1:T(8,128)(2,1)S(1)}, bf16[128,256]{0,1:T(8,128)(2,1)S(1)}, u32[]{:S(2)}, u32[]{:S(2)}) collective-permute-start(bf16[128,256]{0,1:T(8,128)(2,1)S(1)} %collective-permute-done.10), channel_id=1, source_target_pairs={{0,128},{4,132},{8,136},{12,140},{16,144},{20,148},{24,152},{28,15... | collective-permute-start | bytes 196616 | tf_op jit(solution)/shard_map/ppermute | solution.py:23
  411.2 61.0 %all-to-all-start.2 = ((bf16[64,6,2048]{2,1,0:T(8,128)(2,1)}), bf16[64,6,2048]{2,1,0:T(8,128)(2,1)}, u32[]{:S(2)}, u32[]{:S(2)}) async-start(bf16[64,6,2048]{2,1,0:T(8,128)(2,1)} %reshape.329), calls=%async_computation.3 | async-start | bytes 4194304 | tf_op jit(solution)/shard_map/all_to_all | solution.py:173
  422.4 153.8 %reduce-scatter.2.cloned.1.call-start = ((), (), s32[]{:S(2)}) async-start(), calls=%async_computation.5 | async-start | bytes 1310720 | tf_op jit(solution)/shard_map/reduce_scatter | solution.py:164
  461.9 3.0 copy-start.5
  461.9 3.2 copy-start.7
  475.9 100.2 %copy-start.1 = (bf16[1,512,2048]{2,1,0:T(8,128)(2,1)S(1)}, bf16[1,512,2048]{2,1,0:T(8,128)(2,1)}, u32[]{:S(2)}) copy-start(bf16[1,512,2048]{2,1,0:T(8,128)(2,1)} %param.25) | copy-start | bytes 6291460
Sparse Core Ops, SparseCore 0:
  88.4 65.8 all-gather.4
  157.7 89.5 all-gather.2
  464.9 111.1 reduce-scatter.1
where the time goes:
time: 592 us; the launch traced here: 583 us
  waiting for transfers between devices  236 us (40%)
  other arithmetic  89.5 us (15%)
  matrix products  77.4 us (13%)
  blocking collectives  61.3 us (10%)
  starting transfers between devices  58.9 us (10%)
  local copies, waits for them, and re-layouts  43.9 us (7%)
  between operations  14.5 us (2%)
    reduce_scatter x1, waiting for transfers between devices, body(): lax.psum_scatter(jnp.dot(attended, out_weight, preferred_element_type=jnp...  88.3 us
    all_gather x1, waiting for transfers between devices, in_one_piece(): filled, at, done = (lax.all_gather(both, axis, axis=dim, tiled=True), 0, [])  67.3 us
    all_to_all x1, blocking collectives, body(): lax.all_to_all(outbound, 'ep', split_axis=0, concat_axis=0, tiled=True)  61.3 us
    another operation x36, other arithmetic  44.3 us
    ppermute x12, starting transfers between devices, partner(): return lax.ppermute(value, axis, pairs)  42.4 us
    all_gather x1, waiting for transfers between devices, body(): lax.all_gather(arrived.reshape(ep_count * capacity, model_width), 'tp', a...  39.8 us
    ppermute x12, waiting for transfers between devices, partner(): return lax.ppermute(value, axis, pairs)  33.3 us
    dot_general x17, matrix products, visit(): jnp.einsum('rkgd,skd->kgrs', query_rows, key_tile_rows, preferred_element...  32.2 us
  transfers between devices with their start and end apart: 17, of which 14 were waited for; matrix products, arithmetic and copies ran while one was open for 33% of the time, Pallas kernels for 0%

commit v1 on v0

v1 whole, which is shorter than its diff:
```python
import math

import jax
import jax.numpy as jnp
from jax import lax
from jax.experimental import pallas as pl
from jax.experimental.pallas import tpu as pltpu
from jax.sharding import PartitionSpec as P

LOG2E = 1.4426950408889634


def gathered_keys(keys, values, bias, axis):
    rows, kv_heads, head_dim = keys.shape
    kv = jnp.concatenate((keys.reshape(rows, head_dim), values.reshape(rows, head_dim)), axis=1)
    terms = jnp.pad(bias.T, ((0, 16 - bias.shape[1]), (0, 0)))
    return lax.all_gather(jnp.concatenate((kv, terms), axis=0), axis, axis=0, tiled=True)


def mirrored(value, axis):
    count = lax.axis_size(axis)
    return lax.ppermute(value, axis, [(source, count - 1 - source) for source in range(count)])


def split_up(value, dim, length):
    before, after = (value.shape[:dim], value.shape[dim + 1 :])
    return jnp.moveaxis(value.reshape(*before, length, -1, *after), dim, 0)


def summed_on_arrival(value, axis, dim):
    pieces = split_up(value, dim, lax.axis_size(axis))
    arrived = lax.all_to_all(pieces, axis, split_axis=0, concat_axis=0, tiled=True)
    return arrived.astype(jnp.float32).sum(axis=0)


def entry_slots(routes, expert_total):
    flattened_expert_list = routes.reshape(-1)
    onehot = (
        flattened_expert_list[:, None] == jnp.arange(expert_total, dtype=jnp.int32)[None, :]
    ).astype(jnp.int32)
    earlier_count = jnp.cumsum(onehot, axis=0) - onehot
    return (flattened_expert_list, jnp.sum(earlier_count * onehot, axis=1))


def swiglu_rows(piece, gate_cols, up_cols):
    gate_val = jnp.dot(piece, gate_cols, preferred_element_type=jnp.float32)
    up_val = jnp.dot(piece, up_cols, preferred_element_type=jnp.float32)
    return (jax.nn.silu(gate_val) * up_val).astype(jnp.bfloat16)


def attend_kernel(blocks, q_ref, kv_ref, out_ref):
    part = pl.program_id(0)
    heads, half, width = q_ref.shape[1:]
    span = 2 * half
    stride = span + 16
    rows = heads * half
    last = blocks[part]
    q = q_ref[0].reshape(rows, width)
    key_at = lax.broadcasted_iota(jnp.int32, (span, span), 0)
    out_at = lax.broadcasted_iota(jnp.int32, (span, span), 1)
    tri = (key_at >= out_at).astype(jnp.bfloat16)
    scale = LOG2E / math.sqrt(width)

    def scored(block):
        start = pl.multiple_of(block * stride, 16)
        k = kv_ref[pl.ds(start, span), :width]
        raw = lax.dot_general(q, k, (((1,), (1,)), ((), ())), preferred_element_type=jnp.float32)
        terms = kv_ref[pl.ds(start + span, 16), :].astype(jnp.float32) * LOG2E
        bias = jnp.concatenate(
            [jnp.broadcast_to(terms[h : h + 1], (half, span)) for h in range(heads)], axis=0
        )
        return raw * scale + bias

    def summed(scores, earlier):
        soft = jnp.maximum(scores, 0.0) + jnp.log2(1.0 + jnp.exp2(-jnp.abs(scores)))
        if earlier is not None:
            soft = jnp.where(earlier, soft, 0.0)
        high = soft.astype(jnp.bfloat16)
        low = (soft - high.astype(jnp.float32)).astype(jnp.bfloat16)
        return jnp.dot(high, tri, preferred_element_type=jnp.float32) + jnp.dot(
            low, tri, preferred_element_type=jnp.float32
        )

    def added(block, scores, sums, accum, carried, earlier):
        weights = jnp.exp2(scores - sums - carried)
        if earlier is not None:
            weights = jnp.where(earlier, weights, 0.0)
        v = kv_ref[pl.ds(pl.multiple_of(block * stride, 16), span), width:]
        accum = accum + jnp.dot(
            weights.astype(jnp.bfloat16), v, preferred_element_type=jnp.float32
        )
        return accum, carried + sums[:, :1]

    def one(block, state, earlier=None):
        scores = scored(block)
        return added(block, scores, summed(scores, earlier), *state, earlier)

    def two(block, state):
        first, second = scored(block), scored(block - 1)
        first_sums, second_sums = summed(first, None), summed(second, None)
        state = added(block, first, first_sums, *state, None)
        return added(block - 1, second, second_sums, *state, None)

    row_at = lax.broadcasted_iota(jnp.int32, (rows, span), 0) % half + part * half
    earlier = lax.broadcasted_iota(jnp.int32, (rows, span), 1) < row_at
    state = (jnp.zeros((rows, width), jnp.float32), jnp.zeros((rows, 1), jnp.float32))
    state = one(last, state, earlier)
    odd = last % 2
    state = lax.fori_loop(0, odd, lambda i, st: one(last - 1, st), state)
    state = lax.fori_loop(0, last // 2, lambda i, st: two(last - odd - 1 - 2 * i, st), state)
    for h in range(heads):
        out_ref[0, :, h * width : (h + 1) * width] = state[0][h * half : (h + 1) * half].astype(
            jnp.bfloat16
        )


def attend(parts, kv_all, blocks):
    count, heads, half, width = parts.shape
    grid_spec = pltpu.PrefetchScalarGridSpec(
        num_scalar_prefetch=1,
        grid=(count,),
        in_specs=[
            pl.BlockSpec((1, heads, half, width), lambda p, b: (p, 0, 0, 0)),
            pl.BlockSpec(kv_all.shape, lambda p, b: (0, 0), pipeline_mode=pl.Buffered(1)),
        ],
        out_specs=pl.BlockSpec((1, half, heads * width), lambda p, b: (p, 0, 0)),
    )
    pairs = kv_all.shape[0] * heads * half
    return pl.pallas_call(
        attend_kernel,
        grid_spec=grid_spec,
        out_shape=jax.ShapeDtypeStruct((count, half, heads * width), jnp.bfloat16),
        compiler_params=pltpu.CompilerParams(vmem_limit_bytes=40 * 1024 * 1024),
        cost_estimate=pl.CostEstimate(
            flops=pairs * 2048, bytes_accessed=kv_all.size * 2, transcendentals=pairs * 3
        ),
    )(blocks, parts, kv_all)


def body(
    queries,
    keys,
    values,
    key_bias,
    out_weight,
    tokens_b,
    moe_gain,
    gate_weight,
    up_weight,
    down_weight,
    routes,
    route_weights,
):
    tok_rows, local_heads, head_dim = queries.shape
    ep_count = lax.axis_size("ep")
    kv_all = gathered_keys(keys, values, key_bias, "ep")
    device_ep = lax.axis_index("ep")
    half_rows = tok_rows // 2
    by_head = jnp.transpose(queries, (1, 0, 2))
    handed = mirrored(by_head[:, half_rows:], "ep")
    blocks = jnp.stack((device_ep, ep_count - 1 - device_ep)).astype(jnp.int32)
    parts = attend(jnp.stack((by_head[:, :half_rows], handed)), kv_all, blocks)
    attended = jnp.concatenate((parts[0], mirrored(parts[1], "ep")), axis=0)
    tok_b, model_width = tokens_b.shape
    top_count = routes.shape[1]
    expert_total = ep_count * gate_weight.shape[0]
    capacity = max(2, 3 * top_count * tok_b // (2 * expert_total))
    tokens_f = tokens_b.astype(jnp.float32)
    normed = (
        tokens_f
        * lax.rsqrt(jnp.mean(tokens_f * tokens_f, axis=1, keepdims=True) + 1e-06)
        * moe_gain.astype(jnp.float32)
    ).astype(jnp.bfloat16)
    flattened_expert_list, slot_index = entry_slots(routes, expert_total)
    place = flattened_expert_list * capacity + slot_index
    outbound = (
        jnp.zeros((expert_total * capacity, model_width), jnp.bfloat16)
        .at[place]
        .set(jnp.repeat(normed, top_count, axis=0))
    )
    outbound = outbound.reshape(expert_total, capacity, model_width)
    gate_cols = gate_weight[0]
    up_cols = up_weight[0]
    down_rows = down_weight[0]
    arrived = lax.all_to_all(outbound, "ep", split_axis=0, concat_axis=0, tiled=True)
    hidden = swiglu_rows(
        lax.all_gather(arrived.reshape(ep_count * capacity, model_width), "tp", axis=0, tiled=True),
        gate_cols,
        up_cols,
    )
    mixed_sum = summed_on_arrival(
        jnp.dot(attended, out_weight, preferred_element_type=jnp.float32).astype(jnp.bfloat16),
        "tp",
        0,
    ).astype(jnp.bfloat16)
    expert_sum = summed_on_arrival(
        jnp.dot(hidden, down_rows, preferred_element_type=jnp.float32).astype(jnp.bfloat16), "tp", 0
    )
    returned = lax.all_to_all(
        expert_sum.astype(jnp.bfloat16).reshape(ep_count, capacity, model_width),
        "ep",
        split_axis=0,
        concat_axis=0,
        tiled=True,
    )
    picked = jnp.take(returned.reshape(expert_total * capacity, model_width), place, axis=0).astype(
        jnp.float32
    )
    weighted = picked * route_weights.reshape(-1)[:, None]
    moe_out = jnp.sum(weighted.reshape(tok_b, top_count, model_width), axis=1).astype(jnp.bfloat16)
    return (mixed_sum, moe_out)


def solution(mesh):
    in_specs = (
        P("ep", "tp", None),
        P("ep", "tp", None),
        P("ep", "tp", None),
        P("ep", "tp"),
        P("tp", None),
        P(("ep", "tp"), None),
        P(),
        P("ep", None, "tp"),
        P("ep", None, "tp"),
        P("ep", "tp", None),
        P(("ep", "tp"), None),
        P(("ep", "tp"), None),
    )
    out_specs = (P(("ep", "tp"), None), P(("ep", "tp"), None))
    return jax.shard_map(body, mesh=mesh, in_specs=in_specs, out_specs=out_specs, check_vma=False)
```

time: 592 us -> 385 us (0.65)
  other arithmetic: 89.5 us -> 18.2 us
  matrix products: 77.4 us -> 21.7 us
  waiting for transfers between devices: 236 us -> 182 us
  starting transfers between devices: 58.9 us -> 25 us
  Pallas kernels: 0 us -> 27.6 us
  local copies, waits for them, and re-layouts: 43.9 us -> 32.1 us
    reduce_scatter x1 -> x0, waiting for transfers between devices: 88.3 us -> none  [body(): lax.psum_scatter(jnp.dot(attended, out_weight, preferred_element_type=jnp...]
    dot_general x34 -> x0, matrix products: 54.3 us -> none  [the longest x17 32.2 us: visit(): jnp.einsum('rkgd,skd->kgrs', query_rows, key_tile_rows, preferred_element...]
    another operation x36 -> x4, other arithmetic: 44.3 us -> 0.74 us
    all_to_all x1, waiting for transfers between devices: 6.91 us -> 48.4 us  [body(): lax.all_to_all(expert_sum.astype(jnp.bfloat16).reshape(ep_count, capacity...]
    ppermute x12 -> x2, starting transfers between devices: 42.4 us -> 8.72 us  [mirrored(): lax.ppermute(value, axis, [(source, count - 1 - source) for source in ran...]
    pallas_call x0 -> x1, Pallas kernels: none -> 27.6 us  [attend(): pl.pallas_call(attend_kernel, grid_spec=grid_spec, out_shape=jax.ShapeDty...]
    convert_element_type x17 -> x0, other arithmetic: 26.1 us -> none  [visit(): weights = jnp.where(earlier, jnp.exp(jax.nn.log_sigmoid(scores) + after +...]
    all_gather x1, waiting for transfers between devices: 39.8 us -> 65.2 us  [body(): lax.all_gather(arrived.reshape(ep_count * capacity, model_width), 'tp', a...]
  transfers between devices with their start and end apart: 17 -> 7, of which waited for: 14 -> 6; matrix products, arithmetic and copies ran while one was open for 33% -> 9% of each run, Pallas kernels for 0% -> 7%
where the time goes in v1:
time: 385 us; the launch traced here: 382 us
  waiting for transfers between devices  182 us (47%)
  blocking collectives  61.3 us (16%)
  local copies, waits for them, and re-layouts  32.1 us (8%)
  Pallas kernels  27.6 us (7%)
  starting transfers between devices  25 us (6%)
  matrix products  21.7 us (6%)
  other arithmetic  18.2 us (5%)
  between operations  14.2 us (4%)
    all_gather x1, waiting for transfers between devices, body(): lax.all_gather(arrived.reshape(ep_count * capacity, model_width), 'tp', a...  65.2 us
    all_to_all x1, blocking collectives, body(): lax.all_to_all(outbound, 'ep', split_axis=0, concat_axis=0, tiled=True)  61.3 us
    all_gather x1, waiting for transfers between devices, gathered_keys(): lax.all_gather(jnp.concatenate((kv, terms), axis=0), axis, axis=0, tiled=...  50.9 us
    all_to_all x1, waiting for transfers between devices, body(): lax.all_to_all(expert_sum.astype(jnp.bfloat16).reshape(ep_count, capacity...  48.4 us
    pallas_call x1, Pallas kernels, attend(): pl.pallas_call(attend_kernel, grid_spec=grid_spec, out_shape=jax.ShapeDty...  27.6 us
    dot_general x1, matrix products, body(): jnp.dot(hidden, down_rows, preferred_element_type=jnp.float32)  11.7 us
    ppermute x2, waiting for transfers between devices, mirrored(): lax.ppermute(value, axis, [(source, count - 1 - source) for source in ran...  10.8 us
    all_to_all x2, starting transfers between devices, summed_on_arrival(): lax.all_to_all(pieces, axis, split_axis=0, concat_axis=0, tiled=True)  9.48 us
  transfers between devices with their start and end apart: 7, of which 6 were waited for; matrix products, arithmetic and copies ran while one was open for 9% of the time, Pallas kernels for 7%

profile of v1, /device:TPU:64, one launch (start us, length us, event | category | flops | bytes accessed | tf_op | source)
XLA Modules:
  0.0 381.6 jit_solution(4343237595408357428)
XLA Ops:
  7.2 0.9 copy.24
  8.2 0.1 eq.26
  8.3 0.1 reshape.111
  8.4 0.7 broadcast_multiply_fusion
  9.1 0.6 reduce-window.6
  9.7 0.2 slice_reduce_fusion
  10.0 0.1 copy.29
  10.1 0.1 mul.60
  10.2 0.7 convert_element_type.42
  10.9 1.2 fusion.5
  12.2 1.2 fusion.7
  13.4 0.6 broadcast_in_dim.22
  14.0 1.2 reshape.131
  15.3 0.1 fusion.19
  15.4 4.1 %scatter_custom_fusion = bf16[384,2048]{1,0:T(8,128)(2,1)} fusion(s32[256]{0:T(256)S(1)} %bitcast.59, bf16[256,2048]{1,0:T(8,128)(2,1)} %reshape.131, bf16[]{:T(256)} %constant.38.clone.1), kind=kCustom, calls=%fused_computation.17 | custom fusion | bytes 1573376 | tf_op jit(solution)/shard_map/scatter | solution.py:179
  19.5 3.7 reshape.114
  23.2 61.3 %all_to_all.20 = bf16[64,6,2048]{2,1,0:T(8,128)(2,1)} all-to-all(bf16[64,6,2048]{2,1,0:T(8,128)(2,1)} %reshape.114), channel_id=1, replica_groups=mesh['ep'=64,'tp'=4] {'ep'}, dimensions={0} | all-to-all | bytes 3145728 | tf_op jit(solution)/shard_map/all_to_all | solution.py:185
  84.5 3.8 reshape.115
  88.3 0.0 all-gather.3.cloned.1.call-start
  88.4 0.7 fusion.13
  89.1 65.2 %all-gather.5.cloned.1.call-done = bf16[1536,2048]{1,0:T(8,128)(2,1)} async-done(((bf16[384,2048]{1,0:T(8,128)(2,1)}), bf16[1536,2048]{1,0:T(8,128)(2,1)}) %all-gather.5.cloned.1.call-update) | async-done | bytes 6291472 | tf_op jit(solution)/shard_map/all_gather | solution.py:187
  154.3 8.5 %fusion.3 = f32[1536,512]{1,0:T(8,128)} fusion(bf16[1536,2048]{1,0:T(8,128)(2,1)} %all-gather.5.cloned.1.call-done, bf16[1,2048,512]{2,1,0:T(8,128)(2,1)} %param.19), kind=kOutput, calls=%fused_computation.8 | convolution fusion | flops 3221225472 | bytes 11534336 | tf_op jit(solution)/shard_map/dot_general | solution.py:46
  162.9 11.7 %convolution_convert_fusion = bf16[1536,2048]{1,0:T(8,128)(2,1)} fusion(bf16[1,512,2048]{2,1,0:T(8,128)(2,1)S(1)} %copy-done, bf16[1536,2048]{1,0:T(8,128)(2,1)} %all-gather.5.cloned.1.call-done, f32[1536,512]{1,0:T(8,128)} %fusion.3, bf16[1,2048,512]{2,1,0:T(8,128)(2,1)} %param.20), kind=kOutput, calls=%fused_computation.2 | convolution fusion | flops 6450315264 | bytes 19922944 | tf_op jit(solution)/shard_map/dot_general | solution.py:197
  174.6 5.4 %all-to-all-start.2 = ((bf16[4,384,2048]{2,1,0:T(8,128)(2,1)}), bf16[4,384,2048]{2,1,0:T(8,128)(2,1)}, u32[]{:S(2)}, u32[]{:S(2)}) async-start(bf16[4,384,2048]{2,1,0:T(8,128)(2,1)} %bitcast.52), calls=%async_computation.2 | async-start | bytes 12582912 | tf_op jit(solution)/shard_map/all_to_all | solution.py:32
  180.1 5.6 %collective-permute-start = (bf16[2,128,128]{2,1,0:T(8,128)(2,1)S(1)}, bf16[2,128,128]{2,1,0:T(8,128)(2,1)S(1)}, u32[]{:S(2)}, u32[]{:S(2)}) collective-permute-start(bf16[2,128,128]{2,1,0:T(8,128)(2,1)S(1)} %get-tuple-element.5), channel_id=1, source_target_pairs={{0,252},{4,248},{8,244},{12,240},{16,236},{20,232},{24,228},{28,22... | collective-permute-start | bytes 196616 | tf_op jit(solution)/shard_map/ppermute | solution.py:22
  185.7 0.1 pad_add_fusion.blocks
  185.8 4.6 %collective-permute-done = bf16[2,128,128]{2,1,0:T(8,128)(2,1)S(1)} collective-permute-done((bf16[2,128,128]{2,1,0:T(8,128)(2,1)S(1)}, bf16[2,128,128]{2,1,0:T(8,128)(2,1)S(1)}, u32[]{:S(2)}, u32[]{:S(2)}) %collective-permute-start) | collective-permute-done | bytes 65568 | tf_op jit(solution)/shard_map/ppermute | solution.py:22
  190.4 50.9 %all-gather.3.cloned.1.call-done.kv_ref = bf16[17408,256]{1,0:T(8,128)(2,1)} async-done(((bf16[272,256]{1,0:T(8,128)(2,1)}), bf16[17408,256]{1,0:T(8,128)(2,1)}) %all-gather.3.cloned.1.call-update) | async-done | bytes 8912912 | tf_op jit(solution)/shard_map/all_gather | solution.py:17
  241.3 3.5 copy-done.1
  244.9 27.6 %shard_map.131 = bf16[2,128,256]{2,1,0:T(8,128)(2,1)S(1)} custom-call(s32[2]{0:T(128)S(1)} %pad_add_fusion.blocks, bf16[2,2,128,128]{3,2,1,0:T(8,128)(2,1)S(1)} %pad_maximum_fusion.q_ref, bf16[17408,256]{1,0:T(8,128)(2,1)S(1)} %copy-done.1), custom_call_target="tpu_custom_call" | custom-call | flops 9126805504 | bytes 8912896 | tf_op jit(solution)/shard_map/pallas_call | solution.py:129
  272.5 3.1 collective-permute-start.1
  275.6 6.2 %collective-permute-done.1 = bf16[128,256]{1,0:T(8,128)(2,1)S(1)} collective-permute-done((bf16[128,256]{1,0:T(8,128)(2,1)S(1)}, bf16[128,256]{1,0:T(8,128)(2,1)S(1)}, u32[]{:S(2)}, u32[]{:S(2)}) %collective-permute-start.1) | collective-permute-done | bytes 65568 | tf_op jit(solution)/shard_map/ppermute | solution.py:22
  281.7 1.4 convolution_convert_fusion.1
  283.1 4.1 %all-to-all-start = ((bf16[4,64,2048]{2,1,0:T(8,128)(2,1)}), bf16[4,64,2048]{2,1,0:T(8,128)(2,1)S(1)}, u32[]{:S(2)}, u32[]{:S(2)}) async-start(bf16[4,64,2048]{2,1,0:T(8,128)(2,1)} %bitcast.53), calls=%async_computation | async-start | bytes 2097152 | tf_op jit(solution)/shard_map/all_to_all | solution.py:32
  287.2 5.7 %reduce_sum.60 = bf16[384,2048]{1,0:T(8,128)(2,1)} reduce(bf16[4,384,2048]{2,1,0:T(8,128)(2,1)} %all-to-all-done.2, bf16[]{:T(256)} %constant.38.clone.1), dimensions={0}, to_apply=%region_6.7 | reduce | flops 2359296 | bytes 7864322 | tf_op jit(solution)/shard_map/reduce_sum | solution.py:33
  292.9 3.7 reshape.117
  296.6 6.1 %all-to-all-done = bf16[4,64,2048]{2,1,0:T(8,128)(2,1)S(1)} async-done(((bf16[4,64,2048]{2,1,0:T(8,128)(2,1)}), bf16[4,64,2048]{2,1,0:T(8,128)(2,1)S(1)}, u32[]{:S(2)}, u32[]{:S(2)}) %all-to-all-start) | async-done | bytes 1048608 | tf_op jit(solution)/shard_map/all_to_all | solution.py:32
  302.7 6.7 %all-to-all-start.3 = ((bf16[64,6,2048]{2,1,0:T(8,128)(2,1)}), bf16[64,6,2048]{2,1,0:T(8,128)(2,1)}, u32[]{:S(2)}, u32[]{:S(2)}) async-start(bf16[64,6,2048]{2,1,0:T(8,128)(2,1)} %reshape.117), calls=%async_computation.3 | async-start | bytes 4194304 | tf_op jit(solution)/shard_map/all_to_all | solution.py:199
  309.4 0.1 reduce_sum.57
  309.6 0.1 copy.27
  309.7 0.1 copy.28
  309.8 0.1 copy.30
  310.0 0.9 reduce_sum.55
  310.9 48.4 %all-to-all-done.3 = bf16[64,6,2048]{2,1,0:T(8,128)(2,1)} async-done(((bf16[64,6,2048]{2,1,0:T(8,128)(2,1)}), bf16[64,6,2048]{2,1,0:T(8,128)(2,1)}, u32[]{:S(2)}, u32[]{:S(2)}) %all-to-all-start.3) | async-done | bytes 1572896 | tf_op jit(solution)/shard_map/all_to_all | solution.py:199
  359.3 3.7 reshape.118
  363.0 4.0 %gather_fusion = bf16[256,2048]{1,0:T(8,128)(2,1)S(1)} fusion(bf16[384,2048]{1,0:T(8,128)(2,1)} %reshape.118, s32[1024]{0:T(1024)S(1)} %pad_clamp_fusion), kind=kCustom, calls=%fused_computation | custom fusion | bytes 2098176 | tf_op jit(solution)/shard_map/jit(_take)/gather | solution.py:206
  367.0 1.5 gather.7
  368.5 6.2 %multiply_reduce_fusion = bf16[128,2048]{1,0:T(8,128)(2,1)} fusion(bf16[128,2,2048]{2,1,0:T(2,128)(2,1)} %gather.7, pred[128,2]{1,0:T(8,128)(4,1)S(1)} %copy.28, f32[128,2]{1,0:T(8,128)S(1)} %copy.30), kind=kLoop, calls=%fused_computation.10 | loop fusion | flops 1835008 | bytes 1574144 | tf_op jit(solution)/shard_map/reduce_sum | solution.py:210
  (32 shorter events, 0.3 us)
Async XLA Ops:
  7.2 155.7 %copy-start = (bf16[1,512,2048]{2,1,0:T(8,128)(2,1)S(1)}, bf16[1,512,2048]{2,1,0:T(8,128)(2,1)}, u32[]{:S(2)}) copy-start(bf16[1,512,2048]{2,1,0:T(8,128)(2,1)} %param.21) | copy-start | bytes 6291460
  7.2 147.2 %all-gather.5.cloned.1.call-start = ((), (), s32[]{:S(2)}) async-start(), calls=%async_computation.5 | async-start | bytes 7864320 | tf_op jit(solution)/shard_map/all_gather | solution.py:187
  84.5 3.9 %copy-start.4 = (bf16[256,1,128]{2,0,1:T(8,128)(2,1)S(1)}, bf16[256,1,128]{2,0,1:T(8,128)(2,1)}, u32[]{:S(2)}) copy-start(bf16[256,1,128]{2,0,1:T(8,128)(2,1)} %param.14) | copy-start | bytes 196612
  84.5 3.9 %copy-start.5 = (bf16[256,1,128]{2,0,1:T(8,128)(2,1)S(1)}, bf16[256,1,128]{2,0,1:T(8,128)(2,1)}, u32[]{:S(2)}) copy-start(bf16[256,1,128]{2,0,1:T(8,128)(2,1)} %param.13) | copy-start | bytes 196612
  84.5 3.9 %copy-start.7 = (bf16[256,2]{0,1:T(2,128)(2,1)S(1)}, bf16[256,2]{0,1:T(2,128)(2,1)}, u32[]{:S(2)}) copy-start(bf16[256,2]{0,1:T(2,128)(2,1)} %param.15) | copy-start | bytes 3076
  88.3 153.0 %all-gather.3.cloned.1.call-start = ((), (), s32[]{:S(2)}) async-start(), calls=%async_computation.4 | async-start | bytes 9052160 | tf_op jit(solution)/shard_map/all_gather | solution.py:17
  174.6 5.4 %copy-start.3 = (bf16[256,2,128]{2,1,0:T(2,128)(2,1)S(1)}, bf16[256,2,128]{2,1,0:T(2,128)(2,1)}, u32[]{:S(2)}) copy-start(bf16[256,2,128]{2,1,0:T(2,128)(2,1)} %param.12) | copy-start | bytes 393220
  174.6 108.5 %all-to-all-start.2 = ((bf16[4,384,2048]{2,1,0:T(8,128)(2,1)}), bf16[4,384,2048]{2,1,0:T(8,128)(2,1)}, u32[]{:S(2)}, u32[]{:S(2)}) async-start(bf16[4,384,2048]{2,1,0:T(8,128)(2,1)} %bitcast.52), calls=%async_computation.2 | async-start | bytes 12582912 | tf_op jit(solution)/shard_map/all_to_all | solution.py:32
  180.1 10.3 %collective-permute-start = (bf16[2,128,128]{2,1,0:T(8,128)(2,1)S(1)}, bf16[2,128,128]{2,1,0:T(8,128)(2,1)S(1)}, u32[]{:S(2)}, u32[]{:S(2)}) collective-permute-start(bf16[2,128,128]{2,1,0:T(8,128)(2,1)S(1)} %get-tuple-element.5), channel_id=1, source_target_pairs={{0,252},{4,248},{8,244},{12,240},{16,236},{20,232},{24,228},{28,22... | collective-permute-start | bytes 196616 | tf_op jit(solution)/shard_map/ppermute | solution.py:22
  241.3 3.5 copy-start.1
  244.9 36.9 %copy-start.2 = (bf16[256,2048]{1,0:T(8,128)(2,1)S(1)}, bf16[256,2048]{1,0:T(8,128)(2,1)}, u32[]{:S(2)}) copy-start(bf16[256,2048]{1,0:T(8,128)(2,1)} %param.16) | copy-start | bytes 3145732
  272.5 9.3 %collective-permute-start.1 = (bf16[128,256]{1,0:T(8,128)(2,1)S(1)}, bf16[128,256]{1,0:T(8,128)(2,1)S(1)}, u32[]{:S(2)}, u32[]{:S(2)}) collective-permute-start(bf16[128,256]{1,0:T(8,128)(2,1)S(1)} %get-tuple-element.3), channel_id=1, source_target_pairs={{0,252},{4,248},{8,244},{12,240},{16,236},{20,232},{24,228},{28,22... | collective-permute-start | bytes 196616 | tf_op jit(solution)/shard_map/ppermute | solution.py:22
  283.1 19.6 %all-to-all-start = ((bf16[4,64,2048]{2,1,0:T(8,128)(2,1)}), bf16[4,64,2048]{2,1,0:T(8,128)(2,1)S(1)}, u32[]{:S(2)}, u32[]{:S(2)}) async-start(bf16[4,64,2048]{2,1,0:T(8,128)(2,1)} %bitcast.53), calls=%async_computation | async-start | bytes 2097152 | tf_op jit(solution)/shard_map/all_to_all | solution.py:32
  296.6 13.0 %copy-start.6 = (s32[128,2]{0,1:T(2,128)S(1)}, s32[128,2]{0,1:T(2,128)}, u32[]{:S(2)}) copy-start(s32[128,2]{0,1:T(2,128)} %param.22) | copy-start | bytes 3076
  296.6 13.2 %copy-start.8 = (f32[128,2]{0,1:T(2,128)S(1)}, f32[128,2]{0,1:T(2,128)}, u32[]{:S(2)}) copy-start(f32[128,2]{0,1:T(2,128)} %param.23) | copy-start | bytes 3076
  302.7 56.5 %all-to-all-start.3 = ((bf16[64,6,2048]{2,1,0:T(8,128)(2,1)}), bf16[64,6,2048]{2,1,0:T(8,128)(2,1)}, u32[]{:S(2)}, u32[]{:S(2)}) async-start(bf16[64,6,2048]{2,1,0:T(8,128)(2,1)} %reshape.117), calls=%async_computation.3 | async-start | bytes 4194304 | tf_op jit(solution)/shard_map/all_to_all | solution.py:199
Sparse Core Ops, SparseCore 0:
  88.5 65.8 all-gather.4
  157.6 83.6 all-gather.2

commit v2 on v1

--- a/solution.py
+++ b/solution.py
@@ -8,6 +8,12 @@
 from jax.sharding import PartitionSpec as P
 
 LOG2E = 1.4426950408889634
+LANES = 128
+SLABS = 8
+SLAB = 8
+TOP = 2
+CAP = 6
+HELD = 4
 
 
 def gathered_keys(keys, values, bias, axis):
@@ -33,19 +39,418 @@
     return arrived.astype(jnp.float32).sum(axis=0)
 
 
-def entry_slots(routes, expert_total):
-    flattened_expert_list = routes.reshape(-1)
-    onehot = (
-        flattened_expert_list[:, None] == jnp.arange(expert_total, dtype=jnp.int32)[None, :]
-    ).astype(jnp.int32)
-    earlier_count = jnp.cumsum(onehot, axis=0) - onehot
-    return (flattened_expert_list, jnp.sum(earlier_count * onehot, axis=1))
-
-
-def swiglu_rows(piece, gate_cols, up_cols):
-    gate_val = jnp.dot(piece, gate_cols, preferred_element_type=jnp.float32)
-    up_val = jnp.dot(piece, up_cols, preferred_element_type=jnp.float32)
-    return (jax.nn.silu(gate_val) * up_val).astype(jnp.bfloat16)
+def round_step(number):
+    return ((number + 1) // 2) * (2 * (number % 2) - 1)
+
+
+def pack_kernel(routes, place, tokens_ref, gain_ref, out_ref, places_ref, rows_ref, counts):
+    token_count, width = tokens_ref.shape
+    tiles = width // LANES
+    out_ref[...] = jnp.zeros_like(out_ref)
+    tokens = tokens_ref[...].astype(jnp.float32)
+    scale = lax.rsqrt(jnp.mean(tokens * tokens, axis=1, keepdims=True) + 1e-06)
+    normed = tokens * scale * gain_ref[...].astype(jnp.float32)
+    for tile in range(tiles):
+        rows_ref[pl.ds(tile, token_count, stride=tiles), :] = normed[
+            :, tile * LANES : (tile + 1) * LANES
+        ]
+
+    def cleared(index, carry):
+        counts[index] = 0
+        return carry
+
+    lax.fori_loop(0, counts.shape[0], cleared, 0)
+    slab, spot = place[0], place[1]
+
+    def one(token, carry):
+        row = rows_ref[pl.ds(pl.multiple_of(token * tiles, tiles), tiles), :].astype(jnp.bfloat16)
+        for choice in range(TOP):
+            expert = routes[token * TOP + choice]
+            used = counts[expert]
+            counts[expert] = used + 1
+            away = (expert // SLAB - slab + SLABS) % SLABS
+            number = jnp.where(away <= SLABS // 2, jnp.maximum(2 * away - 1, 0), 2 * (SLABS - away))
+            side = (expert % SLAB - spot + SLAB) % SLAB
+            slot = (number * SLAB + side) * CAP + used
+            places_ref[token * TOP + choice] = slot
+            out_ref[pl.ds(pl.multiple_of(slot * tiles, tiles), tiles), :] = row
+        return carry
+
+    lax.fori_loop(0, token_count, one, 0)
+
+
+def packed(tokens, gain, routes, place):
+    token_count, width = tokens.shape
+    tiles = width // LANES
+    return pl.pallas_call(
+        pack_kernel,
+        grid_spec=pltpu.PrefetchScalarGridSpec(
+            num_scalar_prefetch=2,
+            grid=(1,),
+            in_specs=[
+                pl.BlockSpec(tokens.shape, lambda i, r, p: (0, 0)),
+                pl.BlockSpec((1, width), lambda i, r, p: (0, 0)),
+            ],
+            out_specs=[
+                pl.BlockSpec((SLABS * SLAB * CAP * tiles, LANES), lambda i, r, p: (0, 0)),
+                pl.BlockSpec(memory_space=pltpu.SMEM),
+            ],
+            scratch_shapes=[
+                pltpu.VMEM((token_count * tiles, LANES), jnp.float32),
+                pltpu.SMEM((SLABS * SLAB,), jnp.int32),
+            ],
+        ),
+        out_shape=[
+            jax.ShapeDtypeStruct((SLABS * SLAB * CAP * tiles, LANES), jnp.bfloat16),
+            jax.ShapeDtypeStruct((token_count * TOP,), jnp.int32),
+        ],
+        cost_estimate=pl.CostEstimate(flops=10**7, bytes_accessed=2 * 10**6, transcendentals=128),
+        name="pack",
+    )(routes.reshape(-1), place, tokens, gain.reshape(1, -1))
+
+
+def combine_kernel(places, weights, returned_ref, out_ref, rows_ref):
+    token_count, width = out_ref.shape
+    tiles = width // LANES
+
+    def picked(entry):
+        start = pl.multiple_of(places[entry] * tiles, tiles)
+        return returned_ref[pl.ds(start, tiles), :].astype(jnp.float32) * weights[entry]
+
+    def one(token, carry):
+        rows_ref[pl.ds(pl.multiple_of(token * tiles, tiles), tiles), :] = picked(
+            token * TOP
+        ) + picked(token * TOP + 1)
+        return carry
+
+    lax.fori_loop(0, token_count, one, 0)
+    for tile in range(tiles):
+        out_ref[:, tile * LANES : (tile + 1) * LANES] = rows_ref[
+            pl.ds(tile, token_count, stride=tiles), :
+        ].astype(jnp.bfloat16)
+
+
+def combined(returned, places, weights, width):
+    token_count = places.shape[0] // TOP
+    tiles = width // LANES
+    return pl.pallas_call(
+        combine_kernel,
+        grid_spec=pltpu.PrefetchScalarGridSpec(
+            num_scalar_prefetch=2,
+            grid=(1,),
+            in_specs=[pl.BlockSpec(returned.shape, lambda i, p, w: (0, 0))],
+            out_specs=pl.BlockSpec((token_count, width), lambda i, p, w: (0, 0)),
+            scratch_shapes=[pltpu.VMEM((token_count * tiles, LANES), jnp.float32)],
+        ),
+        out_shape=jax.ShapeDtypeStruct((token_count, width), jnp.bfloat16),
+        cost_estimate=pl.CostEstimate(flops=10**7, bytes_accessed=2 * 10**6, transcendentals=0),
+        name="combine",
+    )(places, weights, returned)
+
+
+def expert_kernel(
+    outbound,
+    gate_hbm,
+    up_hbm,
+    down_hbm,
+    out_ref,
+    gate,
+    up,
+    down,
+    arrived,
+    taken,
+    part,
+    opp_out,
+    near_out,
+    far_out,
+    opp_in,
+    near_in,
+    far_in,
+    result,
+    returned,
+    relay,
+    weight_sem,
+    go_send,
+    go_recv,
+    take_send,
+    take_recv,
+    sum_send,
+    sum_recv,
+    back_send,
+    back_recv,
+):
+    me = lax.axis_index("ep")
+    seat = lax.axis_index("tp")
+    seats = lax.axis_size("tp")
+    slab, spot = me // SLAB, me % SLAB
+    width = down.shape[1]
+    tiles = width // LANES
+    block = CAP * tiles
+    group = SLAB * block
+    rows = SLAB * CAP
+
+    def target(number, side):
+        return ((slab + round_step(number) + SLABS) % SLABS) * SLAB + (spot + side) % SLAB
+
+    def origin(number, side):
+        return ((slab - round_step(number) + SLABS) % SLABS) * SLAB + (spot - side + SLAB) % SLAB
+
+    def neighbour(step):
+        return (seat + step + seats) % seats
+
+    def piece(ref, number, side):
+        return ref.at[pl.ds(pl.multiple_of((number * SLAB + side) * block, block), block)]
+
+    def over_ep(source, landing, number, side, device, send, recv):
+        return pltpu.make_async_remote_copy(
+            src_ref=piece(source, number, side),
+            dst_ref=piece(landing, number, side),
+            send_sem=send.at[number],
+            recv_sem=recv.at[number],
+            device_id={"ep": device},
+            device_id_type=pl.DeviceIdType.MESH,
+        )
+
+    def over_tp(source, landing, send, recv, step):
+        return pltpu.make_async_remote_copy(
+            src_ref=source,
+            dst_ref=landing,
+            send_sem=send,
+            recv_sem=recv,
+            device_id={"tp": neighbour(step)},
+            device_id_type=pl.DeviceIdType.MESH,
+        )
+
+    def await_group(ref, sem, number):
+        @pl.when(number == 0)
+        def _():
+            rest = ref.at[pl.ds(block, group - block)]
+            pltpu.make_async_copy(rest, rest, sem.at[0]).wait()
+
+        @pl.when(number > 0)
+        def _():
+            whole = ref.at[pl.ds(pl.multiple_of(number * group, group), group)]
+            pltpu.make_async_copy(whole, whole, sem.at[number]).wait()
+
+    def await_one(ref, sem):
+        pltpu.make_async_copy(ref, ref, sem).wait()
+
+    loads = [
+        pltpu.make_async_copy(source.at[0], landing, weight_sem.at[i])
+        for i, (source, landing) in enumerate(((gate_hbm, gate), (up_hbm, up), (down_hbm, down)))
+    ]
+    for load in loads:
+        load.start()
+
+    barrier = pltpu.get_barrier_semaphore()
+
+    def greet(index, carry):
+        pl.semaphore_signal(
+            barrier,
+            inc=1,
+            device_id={"ep": target(index // SLAB, index % SLAB)},
+            device_id_type=pl.DeviceIdType.MESH,
+        )
+        return carry
+
+    lax.fori_loop(1, SLABS * SLAB, greet, 0)
+    for step in (-1, 1):
+        pl.semaphore_signal(
+            barrier,
+            inc=1,
+            device_id={"tp": neighbour(step)},
+            device_id_type=pl.DeviceIdType.MESH,
+        )
+    pl.semaphore_wait(barrier, SLABS * SLAB + 1)
+
+    def dispatch(index, carry):
+        number, side = index // SLAB, index % SLAB
+        over_ep(
+            outbound, arrived, number, side, target(number, side), go_send, go_recv
+        ).start()
+        return carry
+
+    lax.fori_loop(1, SLABS * SLAB, dispatch, 0)
+    arrived[0:block] = outbound[0:block]
+    for load in loads:
+        load.wait()
+
+    def seat_rows(ref, index, slot):
+        return ref.at[index, pl.ds(pl.multiple_of(slot * rows, rows), rows)]
+
+    def take(number):
+        await_group(arrived, go_recv, number)
+        relay[...] = arrived[pl.ds(pl.multiple_of(number * group, group), group), :].astype(
+            jnp.float32
+        )
+        for tile in range(tiles):
+            taken[number, 0:rows, tile * LANES : (tile + 1) * LANES] = relay[
+                pl.ds(tile, rows, stride=tiles), :
+            ].astype(jnp.bfloat16)
+        for slot, step in ((1, 1), (2, -1)):
+            over_tp(
+                seat_rows(taken, number, 0),
+                seat_rows(taken, number, slot),
+                take_send.at[number, slot - 1],
+                take_recv.at[number, slot],
+                step,
+            ).start()
+
+    def forward(number):
+        odd = number % 2
+        slot = 1 + odd
+        await_one(seat_rows(taken, number, slot), take_recv.at[number, slot])
+        over_tp(
+            seat_rows(taken, number, slot),
+            seat_rows(taken, number, 3),
+            take_send.at[number, 2],
+            take_recv.at[number, 3],
+            1 - 2 * odd,
+        ).start()
+
+    def compute(number):
+        odd = number % 2
+        far = 1 + odd
+        await_one(seat_rows(taken, number, 3 - far), take_recv.at[number, 3 - far])
+        await_one(seat_rows(taken, number, 3), take_recv.at[number, 3])
+        x = taken[number]
+        gated = jnp.dot(x, gate[...], preferred_element_type=jnp.float32)
+        raised = jnp.dot(x, up[...], preferred_element_type=jnp.float32)
+        hidden = (gated / (1.0 + jnp.exp(-gated)) * raised).astype(jnp.bfloat16)
+        held = number % HELD
+        for at in range(0, width, 512):
+            part[held, :, at : at + 512] = jnp.dot(
+                hidden, down[:, at : at + 512], preferred_element_type=jnp.float32
+            )
+        opp_out[number] = part[held, 3 * rows : 4 * rows].astype(jnp.bfloat16)
+        over_tp(
+            opp_out.at[number],
+            opp_in.at[number],
+            sum_send.at[number, 0],
+            sum_recv.at[number, 0],
+            1 - 2 * odd,
+        ).start()
+        far_out[number] = seat_rows(part, held, far)[...].astype(jnp.bfloat16)
+        over_tp(
+            far_out.at[number],
+            far_in.at[number],
+            sum_send.at[number, 1],
+            sum_recv.at[number, 1],
+            2 * odd - 1,
+        ).start()
+
+    def pass_on(number):
+        odd = number % 2
+        await_one(opp_in.at[number], sum_recv.at[number, 0])
+        near_out[number] = (
+            seat_rows(part, number % HELD, 2 - odd)[...] + opp_in[number].astype(jnp.float32)
+        ).astype(jnp.bfloat16)
+        over_tp(
+            near_out.at[number],
+            near_in.at[number],
+            sum_send.at[number, 2],
+            sum_recv.at[number, 2],
+            1 - 2 * odd,
+        ).start()
+
+    def send_back(number):
+        await_one(far_in.at[number], sum_recv.at[number, 1])
+        await_one(near_in.at[number], sum_recv.at[number, 2])
+        for tile in range(tiles):
+            lanes = slice(tile * LANES, (tile + 1) * LANES)
+            relay[pl.ds(tile, rows, stride=tiles), :] = (
+                part[number % HELD, 0:rows, lanes]
+                + far_in[number, :, lanes].astype(jnp.float32)
+                + near_in[number, :, lanes].astype(jnp.float32)
+            )
+        result[pl.ds(pl.multiple_of(number * group, group), group), :] = relay[...].astype(
+            jnp.bfloat16
+        )
+
+        def give(side, carry):
+            over_ep(
+                result, returned, number, side, origin(number, side), back_send, back_recv
+            ).start()
+            return carry
+
+        lax.fori_loop(jnp.where(number == 0, 1, 0), SLAB, give, 0)
+
+    stages = (take, forward, compute, pass_on, send_back)
+
+    def turn(index, carry):
+        for late, stage in enumerate(stages):
+            number = index - late
+
+            @pl.when(jnp.logical_and(number >= 0, number < SLABS))
+            def _(stage=stage, number=number):
+                stage(number)
+
+        return carry
+
+    lax.fori_loop(0, SLABS + len(stages) - 1, turn, 0)
+    returned[0:block] = result[0:block]
+
+    def finish(number, carry):
+        await_group(returned, back_recv, number)
+        await_group(outbound, go_send, number)
+        await_group(result, back_send, number)
+        for index in range(3):
+            await_one(opp_out.at[number], take_send.at[number, index])
+            await_one(opp_out.at[number], sum_send.at[number, index])
+        return carry
+
+    lax.fori_loop(0, SLABS, finish, 0)
+    out_ref[...] = returned[...]
+
+
+def experts(outbound, gate_weight, up_weight, down_weight):
+    width, units = gate_weight.shape[1:]
+    rows = SLAB * CAP
+    tile_rows = outbound.shape[0]
+    shares = (SLABS, rows, width)
+    flat = pltpu.VMEM((tile_rows, LANES), jnp.bfloat16)
+    share = pltpu.VMEM(shares, jnp.bfloat16)
+    dma = pltpu.SemaphoreType.DMA
+    return pl.pallas_call(
+        expert_kernel,
+        out_shape=jax.ShapeDtypeStruct(outbound.shape, jnp.bfloat16),
+        in_specs=[pl.BlockSpec(memory_space=pltpu.VMEM)]
+        + [pl.BlockSpec(memory_space=pl.ANY)] * 3,
+        out_specs=pl.BlockSpec(memory_space=pltpu.VMEM),
+        scratch_shapes=[
+            pltpu.VMEM((width, units), jnp.bfloat16),
+            pltpu.VMEM((width, units), jnp.bfloat16),
+            pltpu.VMEM((units, width), jnp.bfloat16),
+            flat,
+            pltpu.VMEM((SLABS, 4 * rows, width), jnp.bfloat16),
+            pltpu.VMEM((HELD, 4 * rows, width), jnp.float32),
+            share,
+            share,
+            share,
+            share,
+            share,
+            share,
+            flat,
+            flat,
+            pltpu.VMEM((tile_rows // SLABS, LANES), jnp.float32),
+            dma((3,)),
+            dma((SLABS,)),
+            dma((SLABS,)),
+            dma((SLABS, 3)),
+            dma((SLABS, 4)),
+            dma((SLABS, 3)),
+            dma((SLABS, 3)),
+            dma((SLABS,)),
+            dma((SLABS,)),
+        ],
+        compiler_params=pltpu.CompilerParams(
+            collective_id=0, has_side_effects=True, vmem_limit_bytes=60 * 1024 * 1024
+        ),
+        cost_estimate=pl.CostEstimate(
+            flops=8 * tile_rows * LANES * units * 3, bytes_accessed=10**7, transcendentals=10**6
+        ),
+        name="experts",
+    )(outbound, gate_weight, up_weight, down_weight)
 
 
 def attend_kernel(blocks, q_ref, kv_ref, out_ref):
@@ -158,56 +563,20 @@
     half_rows = tok_rows // 2
     by_head = jnp.transpose(queries, (1, 0, 2))
     handed = mirrored(by_head[:, half_rows:], "ep")
+    place = jnp.stack((device_ep // SLAB, device_ep % SLAB)).astype(jnp.int32)
+    outbound, places = packed(tokens_b, moe_gain, routes, place)
+    returned = experts(outbound, gate_weight, up_weight, down_weight)
+    halves = jnp.stack((by_head[:, :half_rows], handed))
+    halves, returned = lax.optimization_barrier((halves, returned))
     blocks = jnp.stack((device_ep, ep_count - 1 - device_ep)).astype(jnp.int32)
-    parts = attend(jnp.stack((by_head[:, :half_rows], handed)), kv_all, blocks)
+    parts = attend(halves, kv_all, blocks)
     attended = jnp.concatenate((parts[0], mirrored(parts[1], "ep")), axis=0)
-    tok_b, model_width = tokens_b.shape
-    top_count = routes.shape[1]
-    expert_total = ep_count * gate_weight.shape[0]
-    capacity = max(2, 3 * top_count * tok_b // (2 * expert_total))
-    tokens_f = tokens_b.astype(jnp.float32)
-    normed = (
-        tokens_f
-        * lax.rsqrt(jnp.mean(tokens_f * tokens_f, axis=1, keepdims=True) + 1e-06)
-        * moe_gain.astype(jnp.float32)
-    ).astype(jnp.bfloat16)
-    flattened_expert_list, slot_index = entry_slots(routes, expert_total)
-    place = flattened_expert_list * capacity + slot_index
-    outbound = (
-        jnp.zeros((expert_total * capacity, model_width), jnp.bfloat16)
-        .at[place]
-        .set(jnp.repeat(normed, top_count, axis=0))
-    )
-    outbound = outbound.reshape(expert_total, capacity, model_width)
-    gate_cols = gate_weight[0]
-    up_cols = up_weight[0]
-    down_rows = down_weight[0]
-    arrived = lax.all_to_all(outbound, "ep", split_axis=0, concat_axis=0, tiled=True)
-    hidden = swiglu_rows(
-        lax.all_gather(arrived.reshape(ep_count * capacity, model_width), "tp", axis=0, tiled=True),
-        gate_cols,
-        up_cols,
-    )
+    moe_out = combined(returned, places, route_weights.reshape(-1), tokens_b.shape[1])
     mixed_sum = summed_on_arrival(
         jnp.dot(attended, out_weight, preferred_element_type=jnp.float32).astype(jnp.bfloat16),
         "tp",
         0,
     ).astype(jnp.bfloat16)
-    expert_sum = summed_on_arrival(
-        jnp.dot(hidden, down_rows, preferred_element_type=jnp.float32).astype(jnp.bfloat16), "tp", 0
-    )
-    returned = lax.all_to_all(
-        expert_sum.astype(jnp.bfloat16).reshape(ep_count, capacity, model_width),
-        "ep",
-        split_axis=0,
-        concat_axis=0,
-        tiled=True,
-    )
-    picked = jnp.take(returned.reshape(expert_total * capacity, model_width), place, axis=0).astype(
-        jnp.float32
-    )
-    weighted = picked * route_weights.reshape(-1)[:, None]
-    moe_out = jnp.sum(weighted.reshape(tok_b, top_count, model_width), axis=1).astype(jnp.bfloat16)
     return (mixed_sum, moe_out)
 
 

time: 385 us -> 248 us (0.64)
  Pallas kernels: 27.6 us -> 191 us
  waiting for transfers between devices: 182 us -> 19 us
  blocking collectives: 61.3 us -> 0 us
  local copies, waits for them, and re-layouts: 32.1 us -> 8.09 us
  matrix products: 21.7 us -> 1.42 us
  other arithmetic: 18.2 us -> 3.3 us
  starting transfers between devices: 25 us -> 10.6 us
    pallas_call x0 -> x3, Pallas kernels: none -> 164 us  [the longest x1 150 us: experts(): pl.pallas_call(expert_kernel, out_shape=jax.ShapeDtypeStruct(outbound.sha...]
    all_gather x1 -> x0, waiting for transfers between devices: 65.2 us -> none  [body(): lax.all_gather(arrived.reshape(ep_count * capacity, model_width), 'tp', a...]
    all_to_all x1 -> x0, blocking collectives: 61.3 us -> none  [body(): lax.all_to_all(outbound, 'ep', split_axis=0, concat_axis=0, tiled=True)]
    all_gather x1, waiting for transfers between devices: 50.9 us -> 0.02 us  [gathered_keys(): lax.all_gather(jnp.concatenate((kv, terms), axis=0), axis, axis=0, tiled=...]
    all_to_all x1 -> x0, waiting for transfers between devices: 48.4 us -> none  [body(): lax.all_to_all(expert_sum.astype(jnp.bfloat16).reshape(ep_count, capacity...]
    dot_general x2 -> x0, matrix products: 20.3 us -> none  [the longest x1 11.7 us: body(): jnp.dot(hidden, down_rows, preferred_element_type=jnp.float32)]
    reshape x6 -> x3, local copies, waits for them, and re-layouts: 16.3 us -> 2.71 us  [the longest x1 1.29 us: packed(): gain.reshape(1, -1)]
    reduce_sum x3 -> x0, other arithmetic: 7.57 us -> none  [the longest x1 6.24 us: body(): jnp.sum(weighted.reshape(tok_b, top_count, model_width), axis=1)]
  transfers between devices with their start and end apart: 7 -> 4, of which waited for: 6 -> 2; matrix products, arithmetic and copies ran while one was open for 9% -> 2% of each run, Pallas kernels for 7% -> 66%
where the time goes in v2:
time: 248 us
  Pallas kernels  191 us (77%)
  waiting for transfers between devices  19 us (8%)
  between operations  14.1 us (6%)
  starting transfers between devices  10.6 us (4%)
  local copies, waits for them, and re-layouts  8.09 us (3%)
  other arithmetic  3.3 us (1%)
    pallas_call x1, Pallas kernels, experts(): pl.pallas_call(expert_kernel, out_shape=jax.ShapeDtypeStruct(outbound.sha...  150 us
    pallas_call x1, Pallas kernels, attend(): pl.pallas_call(attend_kernel, grid_spec=grid_spec, out_shape=jax.ShapeDty...  27.5 us
    all_to_all x1, waiting for transfers between devices, summed_on_arrival(): lax.all_to_all(pieces, axis, split_axis=0, concat_axis=0, tiled=True)  9.74 us
    pallas_call x1, Pallas kernels, packed(): pl.pallas_call(pack_kernel, grid_spec=pltpu.PrefetchScalarGridSpec(num_sc...  9.23 us
    ppermute x2, waiting for transfers between devices, mirrored(): lax.ppermute(value, axis, [(source, count - 1 - source) for source in ran...  9.2 us
    ppermute x2, starting transfers between devices, mirrored(): lax.ppermute(value, axis, [(source, count - 1 - source) for source in ran...  7.01 us
    unnamed x9, local copies, waits for them, and re-layouts  5.36 us
  transfers between devices with their start and end apart: 4, of which 2 were waited for; matrix products, arithmetic and copies ran while one was open for 2% of the time, Pallas kernels for 66%

profile of v2, /device:TPU:64, one launch (start us, length us, event | category | flops | bytes accessed | tf_op | source)
XLA Modules:
  0.0 247.7 jit_solution(5995881925871983559)
XLA Ops:
  7.2 0.0 copy-start
  7.2 0.0 all-gather.2.cloned.1.call-start
  7.2 1.6 fusion.1
  8.9 0.0 all-gather.2.cloned.1.call-update
  8.9 0.9 copy.19
  9.8 6.9 %collective-permute-start = (bf16[2,128,128]{2,1,0:T(8,128)(2,1)S(1)}, bf16[2,128,128]{2,1,0:T(8,128)(2,1)S(1)}, u32[]{:S(2)}, u32[]{:S(2)}) collective-permute-start(bf16[2,128,128]{2,1,0:T(8,128)(2,1)S(1)} %get-tuple-element.13), channel_id=1, source_target_pairs={{0,252},{4,248},{8,244},{12,240},{16,236},{20,232},{24,228},{28,22... | collective-permute-start | bytes 196616 | tf_op jit(solution)/shard_map/ppermute | solution.py:28
  16.8 0.8 copy.16
  17.5 0.7 reshape.22.routes
  18.3 1.3 reshape.23.gain_ref
  19.5 0.7 pad_add_fusion.1.place
  20.2 9.2 %pack.1 = (bf16[6144,128]{1,0:T(8,128)(2,1)}, s32[256]{0:T(256)}) custom-call(s32[256]{0:T(256)} %reshape.22.routes, s32[2]{0:T(128)} %pad_add_fusion.1.place, bf16[128,2048]{1,0:T(8,128)(2,1)} %tokens_ref.1, bf16[1,2048]{1,0:T(2,128)(2,1)} %reshape.23.gain_ref), custom_call_target="tpu_custom_call" | custom-call | flops 10000000 | bytes 2000000 | tf_op jit(solution)/shard_map/pack/pallas_call | solution.py:85
  29.4 149.7 %experts.1.returned_ref = bf16[6144,128]{1,0:T(8,128)(2,1)} custom-call(bf16[6144,128]{1,0:T(8,128)(2,1)} %get-tuple-element.6.outbound, bf16[1,2048,512]{2,1,0:T(8,128)(2,1)} %gate_hbm.1, bf16[1,2048,512]{2,1,0:T(8,128)(2,1)} %up_hbm.1, bf16[1,512,2048]{2,1,0:T(8,128)(2,1)} %down_hbm.1), custom_call_target="tpu_custom_call" | custom-call | flops 9663676416 | bytes 10000000 | tf_op jit(solution)/shard_map/experts/pallas_call | solution.py:414
  179.1 0.1 pad_add_fusion.blocks
  179.2 0.0 collective-permute-done
  179.2 0.0 all-gather.2.cloned.1.call-done.kv_ref
  179.3 0.0 copy-start.1
  179.3 3.5 %copy-done.1 = bf16[17408,256]{1,0:T(8,128)(2,1)S(1)} copy-done((bf16[17408,256]{1,0:T(8,128)(2,1)S(1)}, bf16[17408,256]{1,0:T(8,128)(2,1)}, u32[]{:S(2)}) %copy-start.1) | copy-done | bytes 8912920
  182.8 27.5 %shard_map.131 = bf16[2,128,256]{2,1,0:T(8,128)(2,1)S(1)} custom-call(s32[2]{0:T(128)S(1)} %pad_add_fusion.blocks, bf16[2,2,128,128]{3,2,1,0:T(8,128)(2,1)S(1)} %pad_maximum_fusion.q_ref, bf16[17408,256]{1,0:T(8,128)(2,1)S(1)} %copy-done.1), custom_call_target="tpu_custom_call" | custom-call | flops 9126805504 | bytes 8912896 | tf_op jit(solution)/shard_map/pallas_call | solution.py:534
  210.4 0.1 collective-permute-start.1
  210.5 9.2 %collective-permute-done.1 = bf16[128,256]{1,0:T(8,128)(2,1)S(1)} collective-permute-done((bf16[128,256]{1,0:T(8,128)(2,1)S(1)}, bf16[128,256]{1,0:T(8,128)(2,1)S(1)}, u32[]{:S(2)}, u32[]{:S(2)}) %collective-permute-start.1) | collective-permute-done | bytes 65568 | tf_op jit(solution)/shard_map/ppermute | solution.py:28
  219.7 0.0 copy-done
  219.7 0.0 copy-start.2
  219.7 1.4 convolution_convert_fusion
  221.1 3.5 %all-to-all-start = ((bf16[4,64,2048]{2,1,0:T(8,128)(2,1)}), bf16[4,64,2048]{2,1,0:T(8,128)(2,1)S(1)}, u32[]{:S(2)}, u32[]{:S(2)}) async-start(bf16[4,64,2048]{2,1,0:T(8,128)(2,1)} %bitcast.12), calls=%async_computation | async-start | bytes 2097152 | tf_op jit(solution)/shard_map/all_to_all | solution.py:38
  224.6 0.0 copy-done.2
  224.6 0.1 copy.17
  224.7 0.7 reshape.27.weights
  225.4 4.7 %combine.1 = bf16[128,2048]{1,0:T(8,128)(2,1)} custom-call(s32[256]{0:T(256)} %get-tuple-element.8.places, f32[256]{0:T(256)} %reshape.27.weights, bf16[6144,128]{1,0:T(8,128)(2,1)} %experts.1.returned_ref), custom_call_target="tpu_custom_call" | custom-call | flops 10000000 | bytes 2000000 | tf_op jit(solution)/shard_map/combine/pallas_call | solution.py:136
  230.2 9.7 %all-to-all-done = bf16[4,64,2048]{2,1,0:T(8,128)(2,1)S(1)} async-done(((bf16[4,64,2048]{2,1,0:T(8,128)(2,1)}), bf16[4,64,2048]{2,1,0:T(8,128)(2,1)S(1)}, u32[]{:S(2)}, u32[]{:S(2)}) %all-to-all-start) | async-done | bytes 1048608 | tf_op jit(solution)/shard_map/all_to_all | solution.py:38
  239.9 0.9 reduce_sum.12
  (3 shorter events, 0.0 us)
Async XLA Ops:
  7.2 212.5 %copy-start = (bf16[256,2048]{1,0:T(8,128)(2,1)S(1)}, bf16[256,2048]{1,0:T(8,128)(2,1)}, u32[]{:S(2)}) copy-start(bf16[256,2048]{1,0:T(8,128)(2,1)} %param.16) | copy-start | bytes 3145732
  7.2 172.1 %all-gather.2.cloned.1.call-start = ((), (), s32[]{:S(2)}) async-start(), calls=%async_computation.1 | async-start | bytes 9052160 | tf_op jit(solution)/shard_map/all_gather | solution.py:23
  9.8 169.4 %collective-permute-start = (bf16[2,128,128]{2,1,0:T(8,128)(2,1)S(1)}, bf16[2,128,128]{2,1,0:T(8,128)(2,1)S(1)}, u32[]{:S(2)}, u32[]{:S(2)}) collective-permute-start(bf16[2,128,128]{2,1,0:T(8,128)(2,1)S(1)} %get-tuple-element.13), channel_id=1, source_target_pairs={{0,252},{4,248},{8,244},{12,240},{16,236},{20,232},{24,228},{28,22... | collective-permute-start | bytes 196616 | tf_op jit(solution)/shard_map/ppermute | solution.py:28
  179.3 3.5 %copy-start.1 = (bf16[17408,256]{1,0:T(8,128)(2,1)S(1)}, bf16[17408,256]{1,0:T(8,128)(2,1)}, u32[]{:S(2)}) copy-start(bf16[17408,256]{1,0:T(8,128)(2,1)} %all-gather.2.cloned.1.call-done.kv_ref) | copy-start | bytes 26738692
  210.4 9.3 %collective-permute-start.1 = (bf16[128,256]{1,0:T(8,128)(2,1)S(1)}, bf16[128,256]{1,0:T(8,128)(2,1)S(1)}, u32[]{:S(2)}, u32[]{:S(2)}) collective-permute-start(bf16[128,256]{1,0:T(8,128)(2,1)S(1)} %get-tuple-element.11), channel_id=1, source_target_pairs={{0,252},{4,248},{8,244},{12,240},{16,236},{20,232},{24,228},{28,22... | collective-permute-start | bytes 196616 | tf_op jit(solution)/shard_map/ppermute | solution.py:28
  219.7 4.9 %copy-start.2 = (f32[128,2]{0,1:T(2,128)S(1)}, f32[128,2]{0,1:T(2,128)}, u32[]{:S(2)}) copy-start(f32[128,2]{0,1:T(2,128)} %param.23) | copy-start | bytes 3076
  221.1 18.8 %all-to-all-start = ((bf16[4,64,2048]{2,1,0:T(8,128)(2,1)}), bf16[4,64,2048]{2,1,0:T(8,128)(2,1)S(1)}, u32[]{:S(2)}, u32[]{:S(2)}) async-start(bf16[4,64,2048]{2,1,0:T(8,128)(2,1)} %bitcast.12), calls=%async_computation | async-start | bytes 2097152 | tf_op jit(solution)/shard_map/all_to_all | solution.py:38
Sparse Core Ops, SparseCore 0:
  11.3 92.5 all-gather.1

commit v3 on v2

--- a/solution.py
+++ b/solution.py
@@ -14,6 +14,7 @@
 TOP = 2
 CAP = 6
 HELD = 4
+STEPS = (0, 2, -2, 4, 3, -3, 1, -1)
 
 
 def gathered_keys(keys, values, bias, axis):
@@ -40,7 +41,10 @@
 
 
 def round_step(number):
-    return ((number + 1) // 2) * (2 * (number % 2) - 1)
+    step = 0
+    for at, value in enumerate(STEPS):
+        step = jnp.where(number == at, value, step)
+    return step
 
 
 def pack_kernel(routes, place, tokens_ref, gain_ref, out_ref, places_ref, rows_ref, counts):
@@ -55,28 +59,27 @@
             :, tile * LANES : (tile + 1) * LANES
         ]
 
-    def cleared(index, carry):
-        counts[index] = 0
+    slab, spot = place[0], place[1]
+
+    def opened(index, carry):
+        number, side = index // SLAB, index % SLAB
+        home = ((slab + round_step(number) + SLABS) % SLABS) * SLAB + (spot + side) % SLAB
+        counts[home] = index * CAP
         return carry
 
-    lax.fori_loop(0, counts.shape[0], cleared, 0)
-    slab, spot = place[0], place[1]
+    lax.fori_loop(0, counts.shape[0], opened, 0)
 
     def one(token, carry):
         row = rows_ref[pl.ds(pl.multiple_of(token * tiles, tiles), tiles), :].astype(jnp.bfloat16)
         for choice in range(TOP):
             expert = routes[token * TOP + choice]
-            used = counts[expert]
-            counts[expert] = used + 1
-            away = (expert // SLAB - slab + SLABS) % SLABS
-            number = jnp.where(away <= SLABS // 2, jnp.maximum(2 * away - 1, 0), 2 * (SLABS - away))
-            side = (expert % SLAB - spot + SLAB) % SLAB
-            slot = (number * SLAB + side) * CAP + used
+            slot = counts[expert]
+            counts[expert] = slot + 1
             places_ref[token * TOP + choice] = slot
             out_ref[pl.ds(pl.multiple_of(slot * tiles, tiles), tiles), :] = row
         return carry
 
-    lax.fori_loop(0, token_count, one, 0)
+    lax.fori_loop(0, token_count, one, 0, unroll=4)
 
 
 def packed(tokens, gain, routes, place):
@@ -123,7 +126,7 @@
         ) + picked(token * TOP + 1)
         return carry
 
-    lax.fori_loop(0, token_count, one, 0)
+    lax.fori_loop(0, token_count, one, 0, unroll=4)
     for tile in range(tiles):
         out_ref[:, tile * LANES : (tile + 1) * LANES] = rows_ref[
             pl.ds(tile, token_count, stride=tiles), :
@@ -328,29 +331,29 @@
             opp_in.at[number],
             sum_send.at[number, 0],
             sum_recv.at[number, 0],
-            1 - 2 * odd,
+            2 * odd - 1,
         ).start()
-        far_out[number] = seat_rows(part, held, far)[...].astype(jnp.bfloat16)
+        far_out[number] = seat_rows(part, held, 2 - odd)[...].astype(jnp.bfloat16)
         over_tp(
             far_out.at[number],
             far_in.at[number],
             sum_send.at[number, 1],
             sum_recv.at[number, 1],
-            2 * odd - 1,
+            1 - 2 * odd,
         ).start()
 
     def pass_on(number):
         odd = number % 2
         await_one(opp_in.at[number], sum_recv.at[number, 0])
         near_out[number] = (
-            seat_rows(part, number % HELD, 2 - odd)[...] + opp_in[number].astype(jnp.float32)
+            seat_rows(part, number % HELD, 1 + odd)[...] + opp_in[number].astype(jnp.float32)
         ).astype(jnp.bfloat16)
         over_tp(
             near_out.at[number],
             near_in.at[number],
             sum_send.at[number, 2],
             sum_recv.at[number, 2],
-            1 - 2 * odd,
+            2 * odd - 1,
         ).start()
 
     def send_back(number):

time: 248 us -> 233 us (0.940)
  Pallas kernels: 191 us -> 175 us
    pallas_call x1, Pallas kernels: 150 us -> 137 us  [experts(): pl.pallas_call(expert_kernel, out_shape=jax.ShapeDtypeStruct(outbound.sha...]
    pallas_call x1, Pallas kernels: 9.23 us -> 6.01 us  [packed(): pl.pallas_call(pack_kernel, grid_spec=pltpu.PrefetchScalarGridSpec(num_sc...]
  transfers between devices with their start and end apart: 4 -> 4, of which waited for: 2 -> 2; matrix products, arithmetic and copies ran while one was open for 2% -> 2% of each run, Pallas kernels for 66% -> 64%
where the time goes in v3:
time: 233 us; the launch traced here: 232 us
  Pallas kernels  175 us (75%)
  waiting for transfers between devices  19.7 us (8%)
  between operations  14.1 us (6%)
  starting transfers between devices  10.6 us (5%)
  local copies, waits for them, and re-layouts  8.09 us (3%)
  other arithmetic  3.3 us (1%)
    pallas_call x1, Pallas kernels, experts(): pl.pallas_call(expert_kernel, out_shape=jax.ShapeDtypeStruct(outbound.sha...  137 us
    pallas_call x1, Pallas kernels, attend(): pl.pallas_call(attend_kernel, grid_spec=grid_spec, out_shape=jax.ShapeDty...  27.5 us
    all_to_all x1, waiting for transfers between devices, summed_on_arrival(): lax.all_to_all(pieces, axis, split_axis=0, concat_axis=0, tiled=True)  10.5 us
    ppermute x2, waiting for transfers between devices, mirrored(): lax.ppermute(value, axis, [(source, count - 1 - source) for source in ran...  9.19 us
    ppermute x2, starting transfers between devices, mirrored(): lax.ppermute(value, axis, [(source, count - 1 - source) for source in ran...  7.01 us
    pallas_call x1, Pallas kernels, packed(): pl.pallas_call(pack_kernel, grid_spec=pltpu.PrefetchScalarGridSpec(num_sc...  6.01 us
    unnamed x9, local copies, waits for them, and re-layouts  5.36 us
  transfers between devices with their start and end apart: 4, of which 2 were waited for; matrix products, arithmetic and copies ran while one was open for 2% of the time, Pallas kernels for 64%

profile of v3, /device:TPU:64, one launch (start us, length us, event | category | flops | bytes accessed | tf_op | source)
XLA Modules:
  0.0 232.2 jit_solution(6178266004418823812)
XLA Ops:
  7.2 0.0 copy-start
  7.2 0.0 all-gather.2.cloned.1.call-start
  7.2 1.6 fusion.1
  8.9 0.0 all-gather.2.cloned.1.call-update
  8.9 0.9 copy.19
  9.8 6.9 %collective-permute-start = (bf16[2,128,128]{2,1,0:T(8,128)(2,1)S(1)}, bf16[2,128,128]{2,1,0:T(8,128)(2,1)S(1)}, u32[]{:S(2)}, u32[]{:S(2)}) collective-permute-start(bf16[2,128,128]{2,1,0:T(8,128)(2,1)S(1)} %get-tuple-element.13), channel_id=1, source_target_pairs={{0,252},{4,248},{8,244},{12,240},{16,236},{20,232},{24,228},{28,22... | collective-permute-start | bytes 196616 | tf_op jit(solution)/shard_map/ppermute | solution.py:29
  16.8 0.8 copy.16
  17.5 0.7 reshape.22.routes
  18.3 1.3 reshape.23.gain_ref
  19.5 0.7 pad_add_fusion.1.place
  20.2 6.0 %pack.1 = (bf16[6144,128]{1,0:T(8,128)(2,1)}, s32[256]{0:T(256)}) custom-call(s32[256]{0:T(256)} %reshape.22.routes, s32[2]{0:T(128)} %pad_add_fusion.1.place, bf16[128,2048]{1,0:T(8,128)(2,1)} %tokens_ref.1, bf16[1,2048]{1,0:T(2,128)(2,1)} %reshape.23.gain_ref), custom_call_target="tpu_custom_call" | custom-call | flops 10000000 | bytes 2000000 | tf_op jit(solution)/shard_map/pack/pallas_call | solution.py:88
  26.2 137.5 %experts.1.returned_ref = bf16[6144,128]{1,0:T(8,128)(2,1)} custom-call(bf16[6144,128]{1,0:T(8,128)(2,1)} %get-tuple-element.6.outbound, bf16[1,2048,512]{2,1,0:T(8,128)(2,1)} %gate_hbm.1, bf16[1,2048,512]{2,1,0:T(8,128)(2,1)} %up_hbm.1, bf16[1,512,2048]{2,1,0:T(8,128)(2,1)} %down_hbm.1), custom_call_target="tpu_custom_call" | custom-call | flops 9663676416 | bytes 10000000 | tf_op jit(solution)/shard_map/experts/pallas_call | solution.py:417
  163.7 0.1 pad_add_fusion.blocks
  163.8 0.0 collective-permute-done
  163.8 0.0 all-gather.2.cloned.1.call-done.kv_ref
  163.9 0.0 copy-start.1
  163.9 3.5 %copy-done.1 = bf16[17408,256]{1,0:T(8,128)(2,1)S(1)} copy-done((bf16[17408,256]{1,0:T(8,128)(2,1)S(1)}, bf16[17408,256]{1,0:T(8,128)(2,1)}, u32[]{:S(2)}) %copy-start.1) | copy-done | bytes 8912920
  167.4 27.5 %shard_map.131 = bf16[2,128,256]{2,1,0:T(8,128)(2,1)S(1)} custom-call(s32[2]{0:T(128)S(1)} %pad_add_fusion.blocks, bf16[2,2,128,128]{3,2,1,0:T(8,128)(2,1)S(1)} %pad_maximum_fusion.q_ref, bf16[17408,256]{1,0:T(8,128)(2,1)S(1)} %copy-done.1), custom_call_target="tpu_custom_call" | custom-call | flops 9126805504 | bytes 8912896 | tf_op jit(solution)/shard_map/pallas_call | solution.py:537
  194.9 0.1 collective-permute-start.1
  195.0 9.2 %collective-permute-done.1 = bf16[128,256]{1,0:T(8,128)(2,1)S(1)} collective-permute-done((bf16[128,256]{1,0:T(8,128)(2,1)S(1)}, bf16[128,256]{1,0:T(8,128)(2,1)S(1)}, u32[]{:S(2)}, u32[]{:S(2)}) %collective-permute-start.1) | collective-permute-done | bytes 65568 | tf_op jit(solution)/shard_map/ppermute | solution.py:29
  204.2 0.0 copy-done
  204.2 0.0 copy-start.2
  204.2 1.4 convolution_convert_fusion
  205.7 3.5 %all-to-all-start = ((bf16[4,64,2048]{2,1,0:T(8,128)(2,1)}), bf16[4,64,2048]{2,1,0:T(8,128)(2,1)S(1)}, u32[]{:S(2)}, u32[]{:S(2)}) async-start(bf16[4,64,2048]{2,1,0:T(8,128)(2,1)} %bitcast.12), calls=%async_computation | async-start | bytes 2097152 | tf_op jit(solution)/shard_map/all_to_all | solution.py:39
  209.2 0.0 copy-done.2
  209.2 0.1 copy.17
  209.3 0.7 reshape.27.weights
  210.0 4.0 %combine.1 = bf16[128,2048]{1,0:T(8,128)(2,1)} custom-call(s32[256]{0:T(256)} %get-tuple-element.8.places, f32[256]{0:T(256)} %reshape.27.weights, bf16[6144,128]{1,0:T(8,128)(2,1)} %experts.1.returned_ref), custom_call_target="tpu_custom_call" | custom-call | flops 10000000 | bytes 2000000 | tf_op jit(solution)/shard_map/combine/pallas_call | solution.py:139
  214.0 10.5 %all-to-all-done = bf16[4,64,2048]{2,1,0:T(8,128)(2,1)S(1)} async-done(((bf16[4,64,2048]{2,1,0:T(8,128)(2,1)}), bf16[4,64,2048]{2,1,0:T(8,128)(2,1)S(1)}, u32[]{:S(2)}, u32[]{:S(2)}) %all-to-all-start) | async-done | bytes 1048608 | tf_op jit(solution)/shard_map/all_to_all | solution.py:39
  224.5 0.9 reduce_sum.12
  (3 shorter events, 0.0 us)
Async XLA Ops:
  7.2 197.1 %copy-start = (bf16[256,2048]{1,0:T(8,128)(2,1)S(1)}, bf16[256,2048]{1,0:T(8,128)(2,1)}, u32[]{:S(2)}) copy-start(bf16[256,2048]{1,0:T(8,128)(2,1)} %param.16) | copy-start | bytes 3145732
  7.2 156.7 %all-gather.2.cloned.1.call-start = ((), (), s32[]{:S(2)}) async-start(), calls=%async_computation.1 | async-start | bytes 9052160 | tf_op jit(solution)/shard_map/all_gather | solution.py:24
  9.8 154.0 %collective-permute-start = (bf16[2,128,128]{2,1,0:T(8,128)(2,1)S(1)}, bf16[2,128,128]{2,1,0:T(8,128)(2,1)S(1)}, u32[]{:S(2)}, u32[]{:S(2)}) collective-permute-start(bf16[2,128,128]{2,1,0:T(8,128)(2,1)S(1)} %get-tuple-element.13), channel_id=1, source_target_pairs={{0,252},{4,248},{8,244},{12,240},{16,236},{20,232},{24,228},{28,22... | collective-permute-start | bytes 196616 | tf_op jit(solution)/shard_map/ppermute | solution.py:29
  163.9 3.5 %copy-start.1 = (bf16[17408,256]{1,0:T(8,128)(2,1)S(1)}, bf16[17408,256]{1,0:T(8,128)(2,1)}, u32[]{:S(2)}) copy-start(bf16[17408,256]{1,0:T(8,128)(2,1)} %all-gather.2.cloned.1.call-done.kv_ref) | copy-start | bytes 26738692
  194.9 9.3 %collective-permute-start.1 = (bf16[128,256]{1,0:T(8,128)(2,1)S(1)}, bf16[128,256]{1,0:T(8,128)(2,1)S(1)}, u32[]{:S(2)}, u32[]{:S(2)}) collective-permute-start(bf16[128,256]{1,0:T(8,128)(2,1)S(1)} %get-tuple-element.11), channel_id=1, source_target_pairs={{0,252},{4,248},{8,244},{12,240},{16,236},{20,232},{24,228},{28,22... | collective-permute-start | bytes 196616 | tf_op jit(solution)/shard_map/ppermute | solution.py:29
  204.2 4.9 %copy-start.2 = (f32[128,2]{0,1:T(2,128)S(1)}, f32[128,2]{0,1:T(2,128)}, u32[]{:S(2)}) copy-start(f32[128,2]{0,1:T(2,128)} %param.23) | copy-start | bytes 3076
  205.7 18.8 %all-to-all-start = ((bf16[4,64,2048]{2,1,0:T(8,128)(2,1)}), bf16[4,64,2048]{2,1,0:T(8,128)(2,1)S(1)}, u32[]{:S(2)}, u32[]{:S(2)}) async-start(bf16[4,64,2048]{2,1,0:T(8,128)(2,1)} %bitcast.12), calls=%async_computation | async-start | bytes 2097152 | tf_op jit(solution)/shard_map/all_to_all | solution.py:39
Sparse Core Ops, SparseCore 0:
  11.3 106.3 all-gather.1

commit v4 on v3

--- a/solution.py
+++ b/solution.py
@@ -14,30 +14,18 @@
 TOP = 2
 CAP = 6
 HELD = 4
+LINES = 4
+AHEAD = 3
+ATTEND_FROM = 7
+STEPS_PER_TURN = 7
 STEPS = (0, 2, -2, 4, 3, -3, 1, -1)
 
 
-def gathered_keys(keys, values, bias, axis):
+def key_blocks(keys, values, bias):
     rows, kv_heads, head_dim = keys.shape
     kv = jnp.concatenate((keys.reshape(rows, head_dim), values.reshape(rows, head_dim)), axis=1)
     terms = jnp.pad(bias.T, ((0, 16 - bias.shape[1]), (0, 0)))
-    return lax.all_gather(jnp.concatenate((kv, terms), axis=0), axis, axis=0, tiled=True)
-
-
-def mirrored(value, axis):
-    count = lax.axis_size(axis)
-    return lax.ppermute(value, axis, [(source, count - 1 - source) for source in range(count)])
-
-
-def split_up(value, dim, length):
-    before, after = (value.shape[:dim], value.shape[dim + 1 :])
-    return jnp.moveaxis(value.reshape(*before, length, -1, *after), dim, 0)
-
-
-def summed_on_arrival(value, axis, dim):
-    pieces = split_up(value, dim, lax.axis_size(axis))
-    arrived = lax.all_to_all(pieces, axis, split_axis=0, concat_axis=0, tiled=True)
-    return arrived.astype(jnp.float32).sum(axis=0)
+    return jnp.concatenate((kv, terms), axis=0)
 
 
 def round_step(number):
@@ -151,12 +139,66 @@
     )(places, weights, returned)
 
 
+def attend_block_maker(kv_ref, span, stride, width, rows, locate):
+    half = span // 2
+    key_at = lax.broadcasted_iota(jnp.int32, (span, span), 0)
+    out_at = lax.broadcasted_iota(jnp.int32, (span, span), 1)
+    scale = LOG2E / math.sqrt(width)
+
+    def scored(q, block):
+        start = locate(block)
+        k = kv_ref[pl.ds(start, span), :width]
+        raw = lax.dot_general(q, k, (((1,), (1,)), ((), ())), preferred_element_type=jnp.float32)
+        terms = kv_ref[pl.ds(start + span, 16), :].astype(jnp.float32) * LOG2E
+        bias = jnp.concatenate(
+            [jnp.broadcast_to(terms[h : h + 1], (half, span)) for h in range(rows // half)], axis=0
+        )
+        return raw * scale + bias
+
+    def summed(scores, earlier):
+        soft = jnp.maximum(scores, 0.0) + jnp.log2(1.0 + jnp.exp2(-jnp.abs(scores)))
+        if earlier is not None:
+            soft = jnp.where(earlier, soft, 0.0)
+        high = soft.astype(jnp.bfloat16)
+        low = (soft - high.astype(jnp.float32)).astype(jnp.bfloat16)
+        tri = (key_at >= out_at).astype(jnp.bfloat16)
+        return jnp.dot(high, tri, preferred_element_type=jnp.float32) + jnp.dot(
+            low, tri, preferred_element_type=jnp.float32
+        )
+
+    def added(block, scores, sums, accum, carried, earlier):
+        weights = jnp.exp2(scores - sums - carried)
+        if earlier is not None:
+            weights = jnp.where(earlier, weights, 0.0)
+        v = kv_ref[pl.ds(locate(block), span), width:]
+        accum = accum + jnp.dot(
+            weights.astype(jnp.bfloat16), v, preferred_element_type=jnp.float32
+        )
+        return accum, carried + sums[:, :1]
+
+    def one(q, block, state, earlier=None):
+        scores = scored(q, block)
+        return added(block, scores, summed(scores, earlier), *state, earlier)
+
+    def two(q, block, state):
+        first, second = scored(q, block), scored(q, block - 1)
+        first_sums, second_sums = summed(first, None), summed(second, None)
+        state = added(block, first, first_sums, *state, None)
+        return added(block - 1, second, second_sums, *state, None)
+
+    return one, two
+
+
 def expert_kernel(
     outbound,
+    kv_in,
+    q_in,
+    mix_hbm,
     gate_hbm,
     up_hbm,
     down_hbm,
     out_ref,
+    mixed_ref,
     gate,
     up,
     down,
@@ -172,6 +214,15 @@
     result,
     returned,
     relay,
+    kv_all,
+    q_both,
+    att,
+    att_back,
+    accum,
+    carried,
+    mix_weight,
+    mix_out,
+    mix_in,
     weight_sem,
     go_send,
     go_recv,
@@ -181,6 +232,18 @@
     sum_recv,
     back_send,
     back_recv,
+    col_send,
+    col_recv,
+    row_send,
+    row_recv,
+    hop_send,
+    hop_recv,
+    core_send,
+    core_recv,
+    swap_send,
+    swap_recv,
+    mix_send,
+    mix_recv,
 ):
     me = lax.axis_index("ep")
     seat = lax.axis_index("tp")
@@ -242,6 +305,7 @@
         pltpu.make_async_copy(source.at[0], landing, weight_sem.at[i])
         for i, (source, landing) in enumerate(((gate_hbm, gate), (up_hbm, up), (down_hbm, down)))
     ]
+    loads.append(pltpu.make_async_copy(mix_hbm, mix_weight, weight_sem.at[3]))
     for load in loads:
         load.start()
 
@@ -257,14 +321,14 @@
         return carry
 
     lax.fori_loop(1, SLABS * SLAB, greet, 0)
-    for step in (-1, 1):
+    for step in (-1, 1, 2):
         pl.semaphore_signal(
             barrier,
             inc=1,
             device_id={"tp": neighbour(step)},
             device_id_type=pl.DeviceIdType.MESH,
         )
-    pl.semaphore_wait(barrier, SLABS * SLAB + 1)
+    pl.semaphore_wait(barrier, SLABS * SLAB + 2)
 
     def dispatch(index, carry):
         number, side = index // SLAB, index % SLAB
@@ -273,8 +337,177 @@
         ).start()
         return carry
 
-    lax.fori_loop(1, SLABS * SLAB, dispatch, 0)
+    lax.fori_loop(1, AHEAD * SLAB, dispatch, 0)
+    line, core = spot // 2, spot % 2
+    stride, head_pair = kv_in.shape
+    head_dim = head_pair // 2
+    span = stride - 16
+    half = span // 2
+    mirror = SLABS * SLAB - 1 - me
+
+    def kv_block(core_at, line_at, slab_at):
+        at = (core_at * LINES + line_at) * SLABS + slab_at
+        return kv_all.at[pl.ds(pl.multiple_of(at * stride, 16), stride)]
+
+    def remote(source, landing, send, recv, device):
+        return pltpu.make_async_remote_copy(
+            src_ref=source,
+            dst_ref=landing,
+            send_sem=send,
+            recv_sem=recv,
+            device_id={"ep": device},
+            device_id_type=pl.DeviceIdType.MESH,
+        )
+
+    remote(q_in.at[1], q_both.at[0], swap_send.at[0], swap_recv.at[0], mirror).start()
+    for away in (1, 7, 2, 6, 3, 5, 4):
+        remote(
+            kv_in,
+            kv_block(core, line, slab),
+            col_send.at[away],
+            col_recv.at[away],
+            ((slab + away) % SLABS) * SLAB + spot,
+        ).start()
+    lax.fori_loop(AHEAD * SLAB, SLABS * SLAB, dispatch, 0)
     arrived[0:block] = outbound[0:block]
+    kv_block(core, line, slab)[...] = kv_in[...]
+    q_both[1] = q_in[0]
+
+    def pair_of(number):
+        first = jnp.where(number == 0, 0, SLABS - number)
+        return (slab - first + SLABS) % SLABS, (slab - number - 1 + SLABS) % SLABS
+
+    def on_line(step):
+        return slab * SLAB + ((line + step + LINES) % LINES) * 2 + core
+
+    other_core = slab * SLAB + line * 2 + 1 - core
+
+    def to_core(number, at, line_at, slab_at):
+        held = kv_block(core, line_at, slab_at)
+        remote(
+            held, held, core_send.at[number, at], core_recv.at[number, at], other_core
+        ).start()
+
+    def share_column(number):
+        @pl.when(number > 0)
+        def _():
+            await_one(kv_in, col_recv.at[SLABS - number])
+
+        await_one(kv_in, col_recv.at[number + 1])
+        for which, slab_at in enumerate(pair_of(number)):
+            held = kv_block(core, line, slab_at)
+            for way, step in enumerate((1, -1)):
+                remote(
+                    held,
+                    held,
+                    row_send.at[number, which * 2 + way],
+                    row_recv.at[number, which * 2 + way],
+                    on_line(step),
+                ).start()
+            to_core(number, which, line, slab_at)
+
+    def relay_column(number):
+        for at in range(4):
+            await_one(kv_in, row_recv.at[number, at])
+        left, right = (line - 1 + LINES) % LINES, (line + 1) % LINES
+        first, second = pair_of(number)
+        for way, (line_at, slab_at, step) in enumerate(((left, first, 1), (right, second, -1))):
+            held = kv_block(core, line_at, slab_at)
+            remote(
+                held,
+                held,
+                hop_send.at[number, way],
+                hop_recv.at[number, way],
+                on_line(step),
+            ).start()
+        for at, (line_at, slab_at) in enumerate(
+            ((left, first), (left, second), (right, first), (right, second))
+        ):
+            to_core(number, 2 + at, line_at, slab_at)
+
+    def close_column(number):
+        far_line = (line + 2) % LINES
+        for way, slab_at in enumerate(pair_of(number)):
+            await_one(kv_in, hop_recv.at[number, way])
+            to_core(number, 6 + way, far_line, slab_at)
+
+    def locate(number):
+        at = ((number % 2) * LINES + (number % SLAB) // 2) * SLABS + number // SLAB
+        return pl.multiple_of(at * stride, 16)
+
+    heads = q_in.shape[1] // half
+    one, two = attend_block_maker(kv_all, span, stride, head_dim, heads * half, locate)
+    other_steps = 1 + mirror // 2
+    step_total = SLABS * SLAB // 2 + 1
+
+    def attend_step(number, carry):
+        own = jnp.where(number < other_steps, 0, 1)
+        local = number - own * other_steps
+        last = jnp.where(number < other_steps, mirror, me)
+        odd = last % 2
+        q = q_both[own]
+
+        @pl.when(local == 0)
+        def _():
+            shape = (heads * half, span)
+            row_at = lax.broadcasted_iota(jnp.int32, shape, 0) % half + (1 - own) * half
+            earlier = lax.broadcasted_iota(jnp.int32, shape, 1) < row_at
+            state = (jnp.zeros(accum.shape, jnp.float32), jnp.zeros(carried.shape, jnp.float32))
+            accum[...], carried[...] = one(q, last, state, earlier)
+
+            @pl.when(odd == 1)
+            def _():
+                accum[...], carried[...] = one(q, last - 1, (accum[...], carried[...]))
+
+        @pl.when(local > 0)
+        def _():
+            block_at = last - odd + 1 - 2 * local
+            accum[...], carried[...] = two(q, block_at, (accum[...], carried[...]))
+
+        @pl.when(local == last // 2)
+        def _():
+            for h in range(heads):
+                att[own, :, h * head_dim : (h + 1) * head_dim] = accum[
+                    h * half : (h + 1) * half
+                ].astype(jnp.bfloat16)
+
+        @pl.when(number == other_steps - 1)
+        def _():
+            remote(att.at[0], att_back, swap_send.at[1], swap_recv.at[1], mirror).start()
+
+        return carry
+
+    def attend_some(index):
+        @pl.when(index == ATTEND_FROM)
+        def _():
+            await_one(q_in.at[1], swap_recv.at[0])
+            for number in range(SLABS // 2):
+                for at in range(8):
+                    await_one(kv_in, core_recv.at[number, at])
+
+        first = (index - ATTEND_FROM) * STEPS_PER_TURN
+        lax.fori_loop(first, jnp.minimum(first + STEPS_PER_TURN, step_total), attend_step, 0)
+
+    share = mix_in.shape[1]
+
+    def project(rows_in, at):
+        mix_out[at : at + half] = jnp.dot(
+            rows_in, mix_weight[...], preferred_element_type=jnp.float32
+        ).astype(jnp.bfloat16)
+        for dest in range(at // share, (at + half) // share):
+
+            @pl.when(seat != dest)
+            def _(dest=dest):
+                slot = (seat - dest + seats) % seats - 1
+                pltpu.make_async_remote_copy(
+                    src_ref=mix_out.at[pl.ds(dest * share, share)],
+                    dst_ref=mix_in.at[slot],
+                    send_sem=mix_send.at[slot],
+                    recv_sem=mix_recv.at[slot],
+                    device_id={"tp": dest},
+                    device_id_type=pl.DeviceIdType.MESH,
+                ).start()
+
     for load in loads:
         load.wait()
 
@@ -388,10 +621,42 @@
             def _(stage=stage, number=number):
                 stage(number)
 
+        for late, stage in ((1, share_column), (2, relay_column), (3, close_column)):
+            number = index - late
+
+            @pl.when(jnp.logical_and(number >= 0, number < SLABS // 2))
+            def _(stage=stage, number=number):
+                stage(number)
+
+        @pl.when(index >= ATTEND_FROM)
+        def _():
+            attend_some(index)
+
         return carry
 
     lax.fori_loop(0, SLABS + len(stages) - 1, turn, 0)
     returned[0:block] = result[0:block]
+    project(att[1], 0)
+    await_one(att_back, swap_recv.at[1])
+    project(att_back[...], half)
+    total = mix_out[pl.ds(pl.multiple_of(seat * share, share), share), :].astype(jnp.float32)
+    for slot in range(3):
+        await_one(mix_in.at[slot], mix_recv.at[slot])
+        total = total + mix_in[slot].astype(jnp.float32)
+    mixed_ref[...] = total.astype(jnp.bfloat16)
+    await_one(q_in.at[1], swap_send.at[0])
+    await_one(att_back, swap_send.at[1])
+    for slot in range(3):
+        await_one(mix_in.at[slot], mix_send.at[slot])
+    for away in range(1, SLABS):
+        await_one(kv_in, col_send.at[away])
+    for number in range(SLABS // 2):
+        for at in range(4):
+            await_one(kv_in, row_send.at[number, at])
+        for at in range(2):
+            await_one(kv_in, hop_send.at[number, at])
+        for at in range(8):
+            await_one(kv_in, core_send.at[number, at])
 
     def finish(number, carry):
         await_group(returned, back_recv, number)
@@ -406,8 +671,11 @@
     out_ref[...] = returned[...]
 
 
-def experts(outbound, gate_weight, up_weight, down_weight):
+def experts(outbound, kv_in, q_in, out_weight, gate_weight, up_weight, down_weight):
     width, units = gate_weight.shape[1:]
+    stride = kv_in.shape[0]
+    half = (stride - 16) // 2
+    head_dim = q_in.shape[2]
     rows = SLAB * CAP
     tile_rows = outbound.shape[0]
     shares = (SLABS, rows, width)
@@ -416,10 +684,13 @@
     dma = pltpu.SemaphoreType.DMA
     return pl.pallas_call(
         expert_kernel,
-        out_shape=jax.ShapeDtypeStruct(outbound.shape, jnp.bfloat16),
-        in_specs=[pl.BlockSpec(memory_space=pltpu.VMEM)]
-        + [pl.BlockSpec(memory_space=pl.ANY)] * 3,
-        out_specs=pl.BlockSpec(memory_space=pltpu.VMEM),
+        out_shape=[
+            jax.ShapeDtypeStruct(outbound.shape, jnp.bfloat16),
+            jax.ShapeDtypeStruct((half // 2, width), jnp.bfloat16),
+        ],
+        in_specs=[pl.BlockSpec(memory_space=pltpu.VMEM)] * 3
+        + [pl.BlockSpec(memory_space=pl.ANY)] * 4,
+        out_specs=[pl.BlockSpec(memory_space=pltpu.VMEM)] * 2,
         scratch_shapes=[
             pltpu.VMEM((width, units), jnp.bfloat16),
             pltpu.VMEM((width, units), jnp.bfloat16),
@@ -436,7 +707,16 @@
             flat,
             flat,
             pltpu.VMEM((tile_rows // SLABS, LANES), jnp.float32),
-            dma((3,)),
+            pltpu.VMEM((SLABS * SLAB * stride, 2 * head_dim), jnp.bfloat16),
+            pltpu.VMEM(q_in.shape, jnp.bfloat16),
+            pltpu.VMEM((2, half, 2 * head_dim), jnp.bfloat16),
+            pltpu.VMEM((half, 2 * head_dim), jnp.bfloat16),
+            pltpu.VMEM((2 * half, head_dim), jnp.float32),
+            pltpu.VMEM((2 * half, 1), jnp.float32),
+            pltpu.VMEM(out_weight.shape, jnp.bfloat16),
+            pltpu.VMEM((2 * half, width), jnp.bfloat16),
+            pltpu.VMEM((3, half // 2, width), jnp.bfloat16),
+            dma((4,)),
             dma((SLABS,)),
             dma((SLABS,)),
             dma((SLABS, 3)),
@@ -445,104 +725,27 @@
             dma((SLABS, 3)),
             dma((SLABS,)),
             dma((SLABS,)),
+            dma((SLABS,)),
+            dma((SLABS,)),
+            dma((SLABS // 2, 4)),
+            dma((SLABS // 2, 4)),
+            dma((SLABS // 2, 2)),
+            dma((SLABS // 2, 2)),
+            dma((SLABS // 2, 8)),
+            dma((SLABS // 2, 8)),
+            dma((2,)),
+            dma((2,)),
+            dma((3,)),
+            dma((3,)),
         ],
         compiler_params=pltpu.CompilerParams(
-            collective_id=0, has_side_effects=True, vmem_limit_bytes=60 * 1024 * 1024
+            collective_id=0, has_side_effects=True, vmem_limit_bytes=67043328
         ),
         cost_estimate=pl.CostEstimate(
             flops=8 * tile_rows * LANES * units * 3, bytes_accessed=10**7, transcendentals=10**6
         ),
         name="experts",
-    )(outbound, gate_weight, up_weight, down_weight)
-
-
-def attend_kernel(blocks, q_ref, kv_ref, out_ref):
-    part = pl.program_id(0)
-    heads, half, width = q_ref.shape[1:]
-    span = 2 * half
-    stride = span + 16
-    rows = heads * half
-    last = blocks[part]
-    q = q_ref[0].reshape(rows, width)
-    key_at = lax.broadcasted_iota(jnp.int32, (span, span), 0)
-    out_at = lax.broadcasted_iota(jnp.int32, (span, span), 1)
-    tri = (key_at >= out_at).astype(jnp.bfloat16)
-    scale = LOG2E / math.sqrt(width)
-
-    def scored(block):
-        start = pl.multiple_of(block * stride, 16)
-        k = kv_ref[pl.ds(start, span), :width]
-        raw = lax.dot_general(q, k, (((1,), (1,)), ((), ())), preferred_element_type=jnp.float32)
-        terms = kv_ref[pl.ds(start + span, 16), :].astype(jnp.float32) * LOG2E
-        bias = jnp.concatenate(
-            [jnp.broadcast_to(terms[h : h + 1], (half, span)) for h in range(heads)], axis=0
-        )
-        return raw * scale + bias
-
-    def summed(scores, earlier):
-        soft = jnp.maximum(scores, 0.0) + jnp.log2(1.0 + jnp.exp2(-jnp.abs(scores)))
-        if earlier is not None:
-            soft = jnp.where(earlier, soft, 0.0)
-        high = soft.astype(jnp.bfloat16)
-        low = (soft - high.astype(jnp.float32)).astype(jnp.bfloat16)
-        return jnp.dot(high, tri, preferred_element_type=jnp.float32) + jnp.dot(
-            low, tri, preferred_element_type=jnp.float32
-        )
-
-    def added(block, scores, sums, accum, carried, earlier):
-        weights = jnp.exp2(scores - sums - carried)
-        if earlier is not None:
-            weights = jnp.where(earlier, weights, 0.0)
-        v = kv_ref[pl.ds(pl.multiple_of(block * stride, 16), span), width:]
-        accum = accum + jnp.dot(
-            weights.astype(jnp.bfloat16), v, preferred_element_type=jnp.float32
-        )
-        return accum, carried + sums[:, :1]
-
-    def one(block, state, earlier=None):
-        scores = scored(block)
-        return added(block, scores, summed(scores, earlier), *state, earlier)
-
-    def two(block, state):
-        first, second = scored(block), scored(block - 1)
-        first_sums, second_sums = summed(first, None), summed(second, None)
-        state = added(block, first, first_sums, *state, None)
-        return added(block - 1, second, second_sums, *state, None)
-
-    row_at = lax.broadcasted_iota(jnp.int32, (rows, span), 0) % half + part * half
-    earlier = lax.broadcasted_iota(jnp.int32, (rows, span), 1) < row_at
-    state = (jnp.zeros((rows, width), jnp.float32), jnp.zeros((rows, 1), jnp.float32))
-    state = one(last, state, earlier)
-    odd = last % 2
-    state = lax.fori_loop(0, odd, lambda i, st: one(last - 1, st), state)
-    state = lax.fori_loop(0, last // 2, lambda i, st: two(last - odd - 1 - 2 * i, st), state)
-    for h in range(heads):
-        out_ref[0, :, h * width : (h + 1) * width] = state[0][h * half : (h + 1) * half].astype(
-            jnp.bfloat16
-        )
-
-
-def attend(parts, kv_all, blocks):
-    count, heads, half, width = parts.shape
-    grid_spec = pltpu.PrefetchScalarGridSpec(
-        num_scalar_prefetch=1,
-        grid=(count,),
-        in_specs=[
-            pl.BlockSpec((1, heads, half, width), lambda p, b: (p, 0, 0, 0)),
-            pl.BlockSpec(kv_all.shape, lambda p, b: (0, 0), pipeline_mode=pl.Buffered(1)),
-        ],
-        out_specs=pl.BlockSpec((1, half, heads * width), lambda p, b: (p, 0, 0)),
-    )
-    pairs = kv_all.shape[0] * heads * half
-    return pl.pallas_call(
-        attend_kernel,
-        grid_spec=grid_spec,
-        out_shape=jax.ShapeDtypeStruct((count, half, heads * width), jnp.bfloat16),
-        compiler_params=pltpu.CompilerParams(vmem_limit_bytes=40 * 1024 * 1024),
-        cost_estimate=pl.CostEstimate(
-            flops=pairs * 2048, bytes_accessed=kv_all.size * 2, transcendentals=pairs * 3
-        ),
-    )(blocks, parts, kv_all)
+    )(outbound, kv_in, q_in, out_weight, gate_weight, up_weight, down_weight)
 
 
 def body(
@@ -560,26 +763,20 @@
     route_weights,
 ):
     tok_rows, local_heads, head_dim = queries.shape
-    ep_count = lax.axis_size("ep")
-    kv_all = gathered_keys(keys, values, key_bias, "ep")
     device_ep = lax.axis_index("ep")
-    half_rows = tok_rows // 2
-    by_head = jnp.transpose(queries, (1, 0, 2))
-    handed = mirrored(by_head[:, half_rows:], "ep")
+    halves = jnp.transpose(queries.reshape(2, tok_rows // 2, local_heads, head_dim), (0, 2, 1, 3))
     place = jnp.stack((device_ep // SLAB, device_ep % SLAB)).astype(jnp.int32)
     outbound, places = packed(tokens_b, moe_gain, routes, place)
-    returned = experts(outbound, gate_weight, up_weight, down_weight)
-    halves = jnp.stack((by_head[:, :half_rows], handed))
-    halves, returned = lax.optimization_barrier((halves, returned))
-    blocks = jnp.stack((device_ep, ep_count - 1 - device_ep)).astype(jnp.int32)
-    parts = attend(halves, kv_all, blocks)
-    attended = jnp.concatenate((parts[0], mirrored(parts[1], "ep")), axis=0)
+    returned, mixed_sum = experts(
+        outbound,
+        key_blocks(keys, values, key_bias),
+        halves.reshape(2, -1, head_dim),
+        out_weight,
+        gate_weight,
+        up_weight,
+        down_weight,
+    )
     moe_out = combined(returned, places, route_weights.reshape(-1), tokens_b.shape[1])
-    mixed_sum = summed_on_arrival(
-        jnp.dot(attended, out_weight, preferred_element_type=jnp.float32).astype(jnp.bfloat16),
-        "tp",
-        0,
-    ).astype(jnp.bfloat16)
     return (mixed_sum, moe_out)
 
 

time: 233 us -> 199 us (0.85)
  waiting for transfers between devices: 19.7 us -> 0 us
  between operations: 14.1 us -> 0.68 us
  Pallas kernels: 175 us -> 187 us
  starting transfers between devices: 10.6 us -> 0 us
    pallas_call x2 -> x1, Pallas kernels: 165 us -> 177 us  [experts(): pl.pallas_call(expert_kernel, out_shape=[jax.ShapeDtypeStruct(outbound.sh...]
    all_to_all x1 -> x0, waiting for transfers between devices: 10.5 us -> none  [summed_on_arrival(): lax.all_to_all(pieces, axis, split_axis=0, concat_axis=0, tiled=True)]
    ppermute x2 -> x0, waiting for transfers between devices: 9.19 us -> none  [mirrored(): lax.ppermute(value, axis, [(source, count - 1 - source) for source in ran...]
    ppermute x2 -> x0, starting transfers between devices: 7.01 us -> none  [mirrored(): lax.ppermute(value, axis, [(source, count - 1 - source) for source in ran...]
    all_to_all x1 -> x0, starting transfers between devices: 3.51 us -> none  [summed_on_arrival(): lax.all_to_all(pieces, axis, split_axis=0, concat_axis=0, tiled=True)]
    unnamed x9 -> x5, local copies, waits for them, and re-layouts: 5.36 us -> 2.32 us
  transfers between devices with their start and end apart: 4 -> 0, of which waited for: 2 -> 0; matrix products, arithmetic and copies ran while one was open for 2% -> 0% of each run, Pallas kernels for 64% -> 0%
where the time goes in v4:
time: 199 us; the launch traced here: 197 us
  Pallas kernels  187 us (94%)
  local copies, waits for them, and re-layouts  6.59 us (3%)
  other arithmetic  2.22 us (1%)
    pallas_call x1, Pallas kernels, experts(): pl.pallas_call(expert_kernel, out_shape=[jax.ShapeDtypeStruct(outbound.sh...  177 us
    pallas_call x1, Pallas kernels, packed(): pl.pallas_call(pack_kernel, grid_spec=pltpu.PrefetchScalarGridSpec(num_sc...  6.03 us
    pallas_call x1, Pallas kernels, combined(): pl.pallas_call(combine_kernel, grid_spec=pltpu.PrefetchScalarGridSpec(num...  3.99 us

profile of v4, /device:TPU:64, one launch (start us, length us, event | category | flops | bytes accessed | tf_op | source)
XLA Modules:
  0.0 196.9 jit_solution(12957567430445709790)
XLA Ops:
  0.6 0.7 pad_add_fusion.place
  1.3 0.8 copy.15
  2.1 0.7 reshape.25.routes
  2.8 1.3 reshape.26.gain_ref
  4.1 6.0 %pack.1 = (bf16[6144,128]{1,0:T(8,128)(2,1)}, s32[256]{0:T(256)}) custom-call(s32[256]{0:T(256)} %reshape.25.routes, s32[2]{0:T(128)} %pad_add_fusion.place, bf16[128,2048]{1,0:T(8,128)(2,1)} %tokens_ref.1, bf16[1,2048]{1,0:T(2,128)(2,1)} %reshape.26.gain_ref), custom_call_target="tpu_custom_call" | custom-call | flops 10000000 | bytes 2000000 | tf_op jit(solution)/shard_map/pack/pallas_call | solution.py:76
  10.1 1.6 fusion.1.kv_in
  11.7 1.6 copy.16
  13.3 177.4 %experts.1 = (bf16[6144,128]{1,0:T(8,128)(2,1)}, bf16[64,2048]{1,0:T(8,128)(2,1)}) custom-call(bf16[6144,128]{1,0:T(8,128)(2,1)} %get-tuple-element.6.outbound, bf16[272,256]{1,0:T(8,128)(2,1)} %fusion.1.kv_in, bf16[2,256,128]{2,1,0:T(8,128)(2,1)} %bitcast.10, bf16[256,2048]{1,0:T(8,128)(2,1)} %mix_hbm.1, bf16[1,2048,512]{2,1,0:T(8,128)(2,1)} %gate_hbm.1, ...), custom_call_target="tpu_custom_call" | custom-call | flops 9663676416 | bytes 10000000 | tf_op jit(solution)/shard_map/experts/pallas_call | solution.py:685
  190.7 0.0 copy-start
  190.7 0.8 copy.17
  191.5 0.7 reshape.31.weights
  192.2 4.0 %combine.1 = bf16[128,2048]{1,0:T(8,128)(2,1)} custom-call(s32[256]{0:T(256)} %get-tuple-element.8.places, f32[256]{0:T(256)} %reshape.31.weights, bf16[6144,128]{1,0:T(8,128)(2,1)} %get-tuple-element.9.returned_ref), custom_call_target="tpu_custom_call" | custom-call | flops 10000000 | bytes 2000000 | tf_op jit(solution)/shard_map/combine/pallas_call | solution.py:127
  196.2 0.0 copy-done
  196.2 0.7 copy.19
Async XLA Ops:
  190.7 5.5 %copy-start = (bf16[64,2048]{1,0:T(8,128)(2,1)S(1)}, bf16[64,2048]{1,0:T(8,128)(2,1)}, u32[]{:S(2)}) copy-start(bf16[64,2048]{1,0:T(8,128)(2,1)} %get-tuple-element.12) | copy-start | bytes 786436

commit v5 on v4

--- a/solution.py
+++ b/solution.py
@@ -16,8 +16,9 @@
 HELD = 4
 LINES = 4
 AHEAD = 3
-ATTEND_FROM = 7
+ATTEND_FROM = 5
 STEPS_PER_TURN = 7
+MIX_AT = 10
 STEPS = (0, 2, -2, 4, 3, -3, 1, -1)
 
 
@@ -41,7 +42,8 @@
     out_ref[...] = jnp.zeros_like(out_ref)
     tokens = tokens_ref[...].astype(jnp.float32)
     scale = lax.rsqrt(jnp.mean(tokens * tokens, axis=1, keepdims=True) + 1e-06)
-    normed = tokens * scale * gain_ref[...].astype(jnp.float32)
+    normed = tokens * scale
+    gain = gain_ref[...].astype(jnp.float32)
     for tile in range(tiles):
         rows_ref[pl.ds(tile, token_count, stride=tiles), :] = normed[
             :, tile * LANES : (tile + 1) * LANES
@@ -58,9 +60,10 @@
     lax.fori_loop(0, counts.shape[0], opened, 0)
 
     def one(token, carry):
-        row = rows_ref[pl.ds(pl.multiple_of(token * tiles, tiles), tiles), :].astype(jnp.bfloat16)
+        row = rows_ref[pl.ds(pl.multiple_of(token * tiles, tiles), tiles), :] * gain
+        row = row.astype(jnp.bfloat16)
         for choice in range(TOP):
-            expert = routes[token * TOP + choice]
+            expert = routes[choice, token]
             slot = counts[expert]
             counts[expert] = slot + 1
             places_ref[token * TOP + choice] = slot
@@ -80,7 +83,7 @@
             grid=(1,),
             in_specs=[
                 pl.BlockSpec(tokens.shape, lambda i, r, p: (0, 0)),
-                pl.BlockSpec((1, width), lambda i, r, p: (0, 0)),
+                pl.BlockSpec((tiles, LANES), lambda i, r, p: (0, 0)),
             ],
             out_specs=[
                 pl.BlockSpec((SLABS * SLAB * CAP * tiles, LANES), lambda i, r, p: (0, 0)),
@@ -97,21 +100,21 @@
         ],
         cost_estimate=pl.CostEstimate(flops=10**7, bytes_accessed=2 * 10**6, transcendentals=128),
         name="pack",
-    )(routes.reshape(-1), place, tokens, gain.reshape(1, -1))
+    )(routes.T, place, tokens, gain.reshape(tiles, LANES))
 
 
 def combine_kernel(places, weights, returned_ref, out_ref, rows_ref):
     token_count, width = out_ref.shape
     tiles = width // LANES
 
-    def picked(entry):
-        start = pl.multiple_of(places[entry] * tiles, tiles)
-        return returned_ref[pl.ds(start, tiles), :].astype(jnp.float32) * weights[entry]
+    def picked(token, choice):
+        start = pl.multiple_of(places[token * TOP + choice] * tiles, tiles)
+        return returned_ref[pl.ds(start, tiles), :].astype(jnp.float32) * weights[choice, token]
 
     def one(token, carry):
         rows_ref[pl.ds(pl.multiple_of(token * tiles, tiles), tiles), :] = picked(
-            token * TOP
-        ) + picked(token * TOP + 1)
+            token, 0
+        ) + picked(token, 1)
         return carry
 
     lax.fori_loop(0, token_count, one, 0, unroll=4)
@@ -223,6 +226,8 @@
     mix_weight,
     mix_out,
     mix_in,
+    mix_opp,
+    mix_near,
     weight_sem,
     go_send,
     go_recv,
@@ -321,14 +326,14 @@
         return carry
 
     lax.fori_loop(1, SLABS * SLAB, greet, 0)
-    for step in (-1, 1, 2):
+    for step in (-1, 1):
         pl.semaphore_signal(
             barrier,
             inc=1,
             device_id={"tp": neighbour(step)},
             device_id_type=pl.DeviceIdType.MESH,
         )
-    pl.semaphore_wait(barrier, SLABS * SLAB + 2)
+    pl.semaphore_wait(barrier, SLABS * SLAB + 1)
 
     def dispatch(index, carry):
         number, side = index // SLAB, index % SLAB
@@ -490,23 +495,39 @@
 
     share = mix_in.shape[1]
 
-    def project(rows_in, at):
-        mix_out[at : at + half] = jnp.dot(
-            rows_in, mix_weight[...], preferred_element_type=jnp.float32
+    def seat_share(step):
+        return pl.ds(pl.multiple_of(neighbour(step) * share, share), share)
+
+    def project():
+        mix_out[0:half] = jnp.dot(
+            att[1], mix_weight[...], preferred_element_type=jnp.float32
         ).astype(jnp.bfloat16)
-        for dest in range(at // share, (at + half) // share):
-
-            @pl.when(seat != dest)
-            def _(dest=dest):
-                slot = (seat - dest + seats) % seats - 1
-                pltpu.make_async_remote_copy(
-                    src_ref=mix_out.at[pl.ds(dest * share, share)],
-                    dst_ref=mix_in.at[slot],
-                    send_sem=mix_send.at[slot],
-                    recv_sem=mix_recv.at[slot],
-                    device_id={"tp": dest},
-                    device_id_type=pl.DeviceIdType.MESH,
-                ).start()
+        await_one(att_back, swap_recv.at[1])
+        mix_out[half : 2 * half] = jnp.dot(
+            att_back[...], mix_weight[...], preferred_element_type=jnp.float32
+        ).astype(jnp.bfloat16)
+        for way, step in enumerate((1, -1)):
+            start = neighbour(2) * share + way * (share // 2)
+            over_tp(
+                mix_out.at[pl.ds(pl.multiple_of(start, share // 2), share // 2)],
+                mix_opp.at[way],
+                mix_send.at[way],
+                mix_recv.at[way],
+                step,
+            ).start()
+
+    def add_mixed():
+        for way, step in enumerate((1, -1)):
+            await_one(mix_opp.at[way], mix_recv.at[way])
+            mix_near[way] = mix_out[seat_share(step), :]
+            low = way * (share // 2)
+            high = low + share // 2
+            mix_near[way, low:high] = (
+                mix_near[way, low:high].astype(jnp.float32) + mix_opp[way].astype(jnp.float32)
+            ).astype(jnp.bfloat16)
+            over_tp(
+                mix_near.at[way], mix_in.at[way], mix_send.at[2 + way], mix_recv.at[2 + way], step
+            ).start()
 
     for load in loads:
         load.wait()
@@ -621,10 +642,22 @@
             def _(stage=stage, number=number):
                 stage(number)
 
-        for late, stage in ((1, share_column), (2, relay_column), (3, close_column)):
-            number = index - late
-
-            @pl.when(jnp.logical_and(number >= 0, number < SLABS // 2))
+        for at, stage, number in (
+            (1, share_column, 0),
+            (2, share_column, 1),
+            (2, share_column, 2),
+            (2, relay_column, 0),
+            (3, share_column, 3),
+            (3, relay_column, 1),
+            (3, relay_column, 2),
+            (3, close_column, 0),
+            (4, relay_column, 3),
+            (4, close_column, 1),
+            (4, close_column, 2),
+            (5, close_column, 3),
+        ):
+
+            @pl.when(index == at)
             def _(stage=stage, number=number):
                 stage(number)
 
@@ -632,22 +665,28 @@
         def _():
             attend_some(index)
 
+        @pl.when(index == MIX_AT)
+        def _():
+            project()
+
+        @pl.when(index == MIX_AT + 1)
+        def _():
+            add_mixed()
+
         return carry
 
     lax.fori_loop(0, SLABS + len(stages) - 1, turn, 0)
     returned[0:block] = result[0:block]
-    project(att[1], 0)
-    await_one(att_back, swap_recv.at[1])
-    project(att_back[...], half)
-    total = mix_out[pl.ds(pl.multiple_of(seat * share, share), share), :].astype(jnp.float32)
-    for slot in range(3):
-        await_one(mix_in.at[slot], mix_recv.at[slot])
-        total = total + mix_in[slot].astype(jnp.float32)
+    total = mix_out[seat_share(0), :].astype(jnp.float32)
+    for way in range(2):
+        await_one(mix_in.at[way], mix_recv.at[2 + way])
+        total = total + mix_in[way].astype(jnp.float32)
     mixed_ref[...] = total.astype(jnp.bfloat16)
     await_one(q_in.at[1], swap_send.at[0])
     await_one(att_back, swap_send.at[1])
-    for slot in range(3):
-        await_one(mix_in.at[slot], mix_send.at[slot])
+    for way in range(2):
+        await_one(mix_opp.at[way], mix_send.at[way])
+        await_one(mix_in.at[way], mix_send.at[2 + way])
     for away in range(1, SLABS):
         await_one(kv_in, col_send.at[away])
     for number in range(SLABS // 2):
@@ -715,7 +754,9 @@
             pltpu.VMEM((2 * half, 1), jnp.float32),
             pltpu.VMEM(out_weight.shape, jnp.bfloat16),
             pltpu.VMEM((2 * half, width), jnp.bfloat16),
-            pltpu.VMEM((3, half // 2, width), jnp.bfloat16),
+            pltpu.VMEM((2, half // 2, width), jnp.bfloat16),
+            pltpu.VMEM((2, half // 4, width), jnp.bfloat16),
+            pltpu.VMEM((2, half // 2, width), jnp.bfloat16),
             dma((4,)),
             dma((SLABS,)),
             dma((SLABS,)),
@@ -735,8 +776,8 @@
             dma((SLABS // 2, 8)),
             dma((2,)),
             dma((2,)),
-            dma((3,)),
-            dma((3,)),
+            dma((4,)),
+            dma((4,)),
         ],
         compiler_params=pltpu.CompilerParams(
             collective_id=0, has_side_effects=True, vmem_limit_bytes=67043328
@@ -776,7 +817,7 @@
         up_weight,
         down_weight,
     )
-    moe_out = combined(returned, places, route_weights.reshape(-1), tokens_b.shape[1])
+    moe_out = combined(returned, places, route_weights.T, tokens_b.shape[1])
     return (mixed_sum, moe_out)
 
 

time: 199 us -> 183 us (0.920)
  Pallas kernels: 187 us -> 176 us
  local copies, waits for them, and re-layouts: 6.59 us -> 2.28 us
    pallas_call x1, Pallas kernels: 177 us -> 166 us  [experts(): pl.pallas_call(expert_kernel, out_shape=[jax.ShapeDtypeStruct(outbound.sh...]
    reshape x3 -> x0, local copies, waits for them, and re-layouts: 2.7 us -> none  [the longest x1 1.29 us: packed(): gain.reshape(1, -1)]
where the time goes in v5:
time: 183 us; the launch traced here: 182 us
  Pallas kernels  176 us (96%)
  local copies, waits for them, and re-layouts  2.28 us (1%)
  other arithmetic  2.21 us (1%)
    pallas_call x1, Pallas kernels, experts(): pl.pallas_call(expert_kernel, out_shape=[jax.ShapeDtypeStruct(outbound.sh...  166 us
    pallas_call x1, Pallas kernels, packed(): pl.pallas_call(pack_kernel, grid_spec=pltpu.PrefetchScalarGridSpec(num_sc...  6.03 us
    pallas_call x1, Pallas kernels, combined(): pl.pallas_call(combine_kernel, grid_spec=pltpu.PrefetchScalarGridSpec(num...  4.26 us

profile of v5, /device:TPU:64, one launch (start us, length us, event | category | flops | bytes accessed | tf_op | source)
XLA Modules:
  0.0 181.6 jit_solution(17386498734608827485)
XLA Ops:
  0.6 0.7 pad_add_fusion.place
  1.3 1.6 copy.14
  2.9 1.6 fusion.1.kv_in
  4.4 6.0 %pack.1 = (bf16[6144,128]{1,0:T(8,128)(2,1)}, s32[256]{0:T(256)}) custom-call(s32[2,128]{1,0:T(2,128)} %bitcast.19, s32[2]{0:T(128)} %pad_add_fusion.place, bf16[128,2048]{1,0:T(8,128)(2,1)} %tokens_ref.1, bf16[16,128]{1,0:T(8,128)(2,1)} %bitcast.16), custom_call_target="tpu_custom_call" | custom-call | flops 10000000 | bytes 2000000 | tf_op jit(solution)/shard_map/pack/pallas_call | solution.py:79
  10.5 166.1 %experts.1 = (bf16[6144,128]{1,0:T(8,128)(2,1)}, bf16[64,2048]{1,0:T(8,128)(2,1)}) custom-call(bf16[6144,128]{1,0:T(8,128)(2,1)} %get-tuple-element.6.outbound, bf16[272,256]{1,0:T(8,128)(2,1)} %fusion.1.kv_in, bf16[2,256,128]{2,1,0:T(8,128)(2,1)} %bitcast.13, bf16[256,2048]{1,0:T(8,128)(2,1)} %mix_hbm.1, bf16[1,2048,512]{2,1,0:T(8,128)(2,1)} %gate_hbm.1, ...), custom_call_target="tpu_custom_call" | custom-call | flops 9663676416 | bytes 10000000 | tf_op jit(solution)/shard_map/experts/pallas_call | solution.py:724
  176.6 0.0 copy-start
  176.6 4.3 %combine.1 = bf16[128,2048]{1,0:T(8,128)(2,1)} custom-call(s32[256]{0:T(256)} %get-tuple-element.8.places, f32[2,128]{1,0:T(2,128)} %bitcast.17, bf16[6144,128]{1,0:T(8,128)(2,1)} %get-tuple-element.9.returned_ref), custom_call_target="tpu_custom_call" | custom-call | flops 10000000 | bytes 2000000 | tf_op jit(solution)/shard_map/combine/pallas_call | solution.py:130
  180.9 0.0 copy-done
  180.9 0.7 copy.16
Async XLA Ops:
  176.6 4.3 %copy-start = (bf16[64,2048]{1,0:T(8,128)(2,1)S(1)}, bf16[64,2048]{1,0:T(8,128)(2,1)}, u32[]{:S(2)}) copy-start(bf16[64,2048]{1,0:T(8,128)(2,1)} %get-tuple-element.12) | copy-start | bytes 786436

commit v6 on v5

--- a/solution.py
+++ b/solution.py
@@ -365,15 +365,17 @@
         )
 
     remote(q_in.at[1], q_both.at[0], swap_send.at[0], swap_recv.at[0], mirror).start()
-    for away in (1, 7, 2, 6, 3, 5, 4):
-        remote(
-            kv_in,
-            kv_block(core, line, slab),
-            col_send.at[away],
-            col_recv.at[away],
-            ((slab + away) % SLABS) * SLAB + spot,
-        ).start()
-    lax.fori_loop(AHEAD * SLAB, SLABS * SLAB, dispatch, 0)
+    for ahead, aways in ((AHEAD + 1, (1, 7, 2, 6, 3)), (SLABS, (5, 4))):
+        for away in aways:
+            remote(
+                kv_in,
+                kv_block(core, line, slab),
+                col_send.at[away],
+                col_recv.at[away],
+                ((slab + away) % SLABS) * SLAB + spot,
+            ).start()
+        begin = AHEAD if ahead < SLABS else AHEAD + 1
+        lax.fori_loop(begin * SLAB, ahead * SLAB, dispatch, 0)
     arrived[0:block] = outbound[0:block]
     kv_block(core, line, slab)[...] = kv_in[...]
     q_both[1] = q_in[0]

time: 183 us -> 178 us (0.973)
  Pallas kernels: 176 us -> 172 us
    pallas_call x1, Pallas kernels: 166 us -> 162 us  [experts(): pl.pallas_call(expert_kernel, out_shape=[jax.ShapeDtypeStruct(outbound.sh...]
where the time goes in v6:
time: 178 us; the launch traced here: 177 us
  Pallas kernels  172 us (97%)
  local copies, waits for them, and re-layouts  2.28 us (1%)
  other arithmetic  2.21 us (1%)
    pallas_call x1, Pallas kernels, experts(): pl.pallas_call(expert_kernel, out_shape=[jax.ShapeDtypeStruct(outbound.sh...  162 us
    pallas_call x1, Pallas kernels, packed(): pl.pallas_call(pack_kernel, grid_spec=pltpu.PrefetchScalarGridSpec(num_sc...  6.03 us
    pallas_call x1, Pallas kernels, combined(): pl.pallas_call(combine_kernel, grid_spec=pltpu.PrefetchScalarGridSpec(num...  4.26 us

profile of v6, /device:TPU:64, one launch (start us, length us, event | category | flops | bytes accessed | tf_op | source)
XLA Modules:
  0.0 177.1 jit_solution(4096217030380156355)
XLA Ops:
  0.6 0.7 pad_add_fusion.place
  1.3 1.6 copy.14
  2.9 1.6 fusion.1.kv_in
  4.4 6.0 %pack.1 = (bf16[6144,128]{1,0:T(8,128)(2,1)}, s32[256]{0:T(256)}) custom-call(s32[2,128]{1,0:T(2,128)} %bitcast.19, s32[2]{0:T(128)} %pad_add_fusion.place, bf16[128,2048]{1,0:T(8,128)(2,1)} %tokens_ref.1, bf16[16,128]{1,0:T(8,128)(2,1)} %bitcast.16), custom_call_target="tpu_custom_call" | custom-call | flops 10000000 | bytes 2000000 | tf_op jit(solution)/shard_map/pack/pallas_call | solution.py:79
  10.5 161.6 %experts.1 = (bf16[6144,128]{1,0:T(8,128)(2,1)}, bf16[64,2048]{1,0:T(8,128)(2,1)}) custom-call(bf16[6144,128]{1,0:T(8,128)(2,1)} %get-tuple-element.6.outbound, bf16[272,256]{1,0:T(8,128)(2,1)} %fusion.1.kv_in, bf16[2,256,128]{2,1,0:T(8,128)(2,1)} %bitcast.13, bf16[256,2048]{1,0:T(8,128)(2,1)} %mix_hbm.1, bf16[1,2048,512]{2,1,0:T(8,128)(2,1)} %gate_hbm.1, ...), custom_call_target="tpu_custom_call" | custom-call | flops 9663676416 | bytes 10000000 | tf_op jit(solution)/shard_map/experts/pallas_call | solution.py:726
  172.1 0.0 copy-start
  172.1 4.3 %combine.1 = bf16[128,2048]{1,0:T(8,128)(2,1)} custom-call(s32[256]{0:T(256)} %get-tuple-element.8.places, f32[2,128]{1,0:T(2,128)} %bitcast.17, bf16[6144,128]{1,0:T(8,128)(2,1)} %get-tuple-element.9.returned_ref), custom_call_target="tpu_custom_call" | custom-call | flops 10000000 | bytes 2000000 | tf_op jit(solution)/shard_map/combine/pallas_call | solution.py:130
  176.4 0.0 copy-done
  176.4 0.7 copy.16
Async XLA Ops:
  172.1 4.3 %copy-start = (bf16[64,2048]{1,0:T(8,128)(2,1)S(1)}, bf16[64,2048]{1,0:T(8,128)(2,1)}, u32[]{:S(2)}) copy-start(bf16[64,2048]{1,0:T(8,128)(2,1)} %get-tuple-element.12) | copy-start | bytes 786436
